TPU v7x, 32 devices: a whole 2x2x4 slice. The times are simulated.
32 devices in a mesh: sp: 16 (over z, y, core), tp: 2 (over x).
Axes of the slice: x: 2, y: 2, z: 4, core: 2. Of those that a mesh axis runs over, the one named last changes fastest.
Arguments:
- queries: bfloat16 [8192, 1024], P('sp', 'tp'), may hold values from -160 to 160
- keys: bfloat16 [8192, 256], P('sp', 'tp'), may hold values from -5 to 5
- values: bfloat16 [8192, 256], P('sp', 'tp'), may hold values from -6 to 6
- doc_ids: int32 [8192], P('sp'), may hold values from 0 to 7, never falling along the last dimension, each value on 1 to 2048 neighbouring positions
- sink_logit: float32 [16], P('tp'), may hold values from 1 to 6
- w_out: bfloat16 [1024, 2048], P('tp'), may hold values from -0.1875 to 0.1875
- residual: bfloat16 [8192, 2048], P(('sp', 'tp')), may hold values from -6 to 6
- ffn_gain: float32 [2048], replicated, may hold values from 0.1 to 1.9
- expert_ids: int32 [8192, 8], P(('sp', 'tp')), may hold values from 0 to 15, all different within a row; in each aligned block of 128 rows (0 to 127, 128 to 255, ...) at most 96 rows name the same one
- expert_weight: float32 [8192, 8], P(('sp', 'tp')), may hold values from 0.2 to 2
- exp_gate: bfloat16 [16, 2048, 512], P('sp'), may hold values from -0.125 to 0.125
- exp_up: bfloat16 [16, 2048, 512], P('sp'), may hold values from -0.125 to 0.125
- exp_down: bfloat16 [16, 512, 2048], P('sp'), may hold values from -0.25 to 0.25
- shared_gate: bfloat16 [2048, 512], P(None, 'tp'), may hold values from -0.125 to 0.125
- shared_up: bfloat16 [2048, 512], P(None, 'tp'), may hold values from -0.125 to 0.125
- shared_down: bfloat16 [512, 2048], P('tp'), may hold values from -0.25 to 0.25
Outputs:
- output: bfloat16 [8192, 2048], P(('sp', 'tp'))
Inputs may be any that keep to these rules, and one draw needn't show every extreme that they name: `doc_ids`: never falling along the sequence; every document holds at most 2048 positions, and one holds exactly that many. `expert_ids`: each row names 8 different experts. In each aligned block of 128 rows no expert is named by more than 96 rows, and in some blocks one expert is named by exactly 96 rows.
All inputs are finite; a program needn't handle non-finite values.
Results may differ from a plain program's by a relative error of at most 0.018.
Values may be sent and summed in bfloat16 or wider, within the bound.
A program may use at most 128 MiB of HBM per device.

v0:
```python
import math

import jax
import jax.numpy as jnp
from jax import lax
from jax.experimental import pallas as pl
from jax.experimental.pallas import tpu as pltpu
from jax.sharding import PartitionSpec as P

HD = 64
WINDOW = 128
PARTS = 2


norm_eps = 1e-06


def extended(cells, sides, width):
    for axis, dim in sides:
        count = lax.axis_size(axis)
        ends = count - 1
        head = lax.slice_in_dim(cells, 0, width, axis=dim)
        tail = lax.slice_in_dim(cells, cells.shape[dim] - width, cells.shape[dim], axis=dim)
        cells = jnp.concatenate(
            [
                lax.ppermute(tail, axis, [(i, (i + 1) % count) for i in range(ends)]),
                cells,
                lax.ppermute(head, axis, [((i + 1) % count, i) for i in range(ends)]),
            ],
            axis=dim,
        )
    return cells


def band_blocks(padded, width):
    span_count = padded.shape[0] // width - 2
    shaped = padded.reshape((span_count + 2, width) + padded.shape[1:])
    return jnp.concatenate(
        [
            shaped[0:span_count:2],
            shaped[1 : span_count + 1 : 2],
            shaped[2 : span_count + 2 : 2],
            shaped[3 : span_count + 3 : 2],
        ],
        axis=1,
    )


def attend(queries, ext_keys, ext_values, ext_marks, own_marks, sink_logit):
    tok_count = queries.shape[0]
    head_count = sink_logit.shape[0]
    key_heads = ext_keys.shape[1] // HD
    group_size = head_count // key_heads
    query_span = 2 * WINDOW
    block_count = tok_count // query_span
    query_blocks = queries.reshape(block_count, query_span, key_heads, group_size, HD)
    key_blocks = band_blocks(ext_keys, WINDOW).reshape(block_count, 4 * WINDOW, key_heads, HD)
    value_blocks = band_blocks(ext_values, WINDOW).reshape(block_count, 4 * WINDOW, key_heads, HD)
    mark_blocks = band_blocks(ext_marks, WINDOW)
    query_marks = own_marks.reshape(block_count, query_span)
    scores = jnp.einsum(
        "nqkgd,nmkd->nkgqm", query_blocks, key_blocks, preferred_element_type=jnp.float32
    ) * HD ** (-0.5)
    offset = (
        jnp.arange(query_span, dtype=jnp.int32)[:, None]
        - jnp.arange(4 * WINDOW, dtype=jnp.int32)[None, :]
        + WINDOW
    )
    allowed = (jnp.abs(offset) <= WINDOW)[None] & (
        mark_blocks[:, None, :] == query_marks[:, :, None]
    )
    scores = jnp.where(allowed[:, None, None], scores, -jnp.inf)
    sink_term = sink_logit.reshape(key_heads, group_size)[None, :, :, None, None]
    row_max = jnp.maximum(jnp.max(scores, axis=-1, keepdims=True), sink_term)
    exp_scores = jnp.exp(scores - row_max)
    attn_probs = (
        exp_scores / (jnp.sum(exp_scores, axis=-1, keepdims=True) + jnp.exp(sink_term - row_max))
    ).astype(jnp.bfloat16)
    result = jnp.einsum(
        "nkgqm,nmkd->nqkgd", attn_probs, value_blocks, preferred_element_type=jnp.float32
    )
    return result.astype(jnp.bfloat16).reshape(tok_count, head_count * HD)


def expert_kernel(rows_ref, scale_ref, gate_ref, up_ref, down_ref, side_ref, side_down_ref, out_ref):
    rows = rows_ref[...]
    gated = jnp.dot(rows, gate_ref[...], preferred_element_type=jnp.float32)
    lifted = jnp.dot(rows, up_ref[...], preferred_element_type=jnp.float32)
    hidden = (gated / (1.0 + jnp.exp(-gated)) * lifted).astype(jnp.bfloat16)
    produced = jnp.dot(hidden, down_ref[...], preferred_element_type=jnp.float32)
    side = jnp.dot(rows, side_ref[...], preferred_element_type=jnp.float32)
    width = side.shape[1] // 2
    side_gate, side_up = side[:, :width], side[:, width:]
    side_hidden = (side_gate / (1.0 + jnp.exp(-side_gate)) * side_up).astype(jnp.bfloat16)
    shared = jnp.dot(side_hidden, side_down_ref[...], preferred_element_type=jnp.float32)
    out_ref[...] = (
        scale_ref[...] * produced.astype(jnp.bfloat16).astype(jnp.float32) + shared
    ).astype(jnp.bfloat16)


def run_experts(rows, scale, gate_w, up_w, down_w, side_w, side_down):
    count, width = rows.shape
    tile = math.gcd(count, 256)
    whole = lambda w: pl.BlockSpec(w.shape, lambda i: (0, 0))
    units = gate_w.shape[1] + side_w.shape[1] // 2
    return pl.pallas_call(
        expert_kernel,
        grid=(count // tile,),
        in_specs=[
            pl.BlockSpec((tile, width), lambda i: (i, 0)),
            pl.BlockSpec((tile, 1), lambda i: (i, 0)),
            whole(gate_w),
            whole(up_w),
            whole(down_w),
            whole(side_w),
            whole(side_down),
        ],
        out_specs=pl.BlockSpec((tile, width), lambda i: (i, 0)),
        out_shape=jax.ShapeDtypeStruct((count, width), jnp.bfloat16),
        compiler_params=pltpu.CompilerParams(
            dimension_semantics=("arbitrary",), vmem_limit_bytes=48 * 1024 * 1024
        ),
        cost_estimate=pl.CostEstimate(
            flops=6 * count * width * units,
            bytes_accessed=4 * count * width + 6 * units * width,
            transcendentals=count * units,
        ),
    )(rows, scale, gate_w, up_w, down_w, side_w, side_down)


def shared_slice(shared_gate, shared_up, shared_down):
    sp_count, tp_count = lax.axis_size("sp"), lax.axis_size("tp")
    own, side = lax.axis_index("tp"), lax.axis_index("sp")
    units = shared_gate.shape[1] * tp_count // sp_count
    per_owner = sp_count // tp_count
    owner, offset = side // per_owner, (side % per_owner) * units
    held = jnp.concatenate(
        [
            lax.dynamic_slice_in_dim(shared_gate, offset, units, axis=1).T,
            lax.dynamic_slice_in_dim(shared_up, offset, units, axis=1).T,
            lax.dynamic_slice_in_dim(shared_down, offset, units, axis=0),
        ],
        axis=0,
    )
    chosen = held
    for shift in range(1, tp_count):
        came = lax.ppermute(held, "tp", [(i, (i + shift) % tp_count) for i in range(tp_count)])
        chosen = jnp.where((own - shift) % tp_count == owner, came, chosen)
    padded = -(-units // 128) * 128
    grown = [
        jnp.pad(chosen[i * units : (i + 1) * units], ((0, padded - units), (0, 0))) for i in range(3)
    ]
    return jnp.concatenate(grown[:2], axis=0).T, grown[2]


def shards(
    queries,
    keys,
    values,
    doc_ids,
    sink_logit,
    w_out,
    residual,
    ffn_gain,
    expert_ids,
    expert_weight,
    exp_gate,
    exp_up,
    exp_down,
    shared_gate,
    shared_up,
    shared_down,
):
    marks = (doc_ids + 1).astype(jnp.bfloat16)
    kv = keys.shape[1]
    joined = jnp.concatenate(
        [keys, values, jnp.broadcast_to(marks[:, None], (marks.shape[0], 128))], axis=1
    )
    extended_all = extended(joined, (("sp", 0),), WINDOW)
    ext_keys, ext_values, ext_marks = (
        extended_all[:, :kv],
        extended_all[:, kv : 2 * kv],
        extended_all[:, 2 * kv],
    )
    attended = attend(queries, ext_keys, ext_values, ext_marks, marks, sink_logit)
    row_count = residual.shape[0]
    mixed = lax.psum_scatter(
        jnp.dot(attended, w_out, preferred_element_type=jnp.float32).astype(jnp.bfloat16),
        "tp",
        scatter_dimension=0,
        tiled=True,
    ).astype(jnp.float32)
    resid = (residual.astype(jnp.float32) + mixed).astype(jnp.bfloat16)
    resid_f = resid.astype(jnp.float32)
    normed = (
        resid_f
        * lax.rsqrt(jnp.mean(resid_f * resid_f, axis=-1, keepdims=True) + norm_eps)
        * ffn_gain
    ).astype(jnp.bfloat16)
    side_w, side_down = shared_slice(shared_gate, shared_up, shared_down)
    sp_count = lax.axis_size("sp")
    chosen = expert_ids[:, :, None] == jnp.arange(sp_count, dtype=jnp.int32)
    table = jnp.sum(jnp.where(chosen, expert_weight[:, :, None], 0.0), axis=1)
    scales = lax.all_to_all(table.T, "sp", split_axis=0, concat_axis=0, tiled=True)
    part_rows = row_count // PARTS
    sums = []
    for part in range(PARTS):
        begin = part * part_rows
        gathered = lax.all_gather(normed[begin : begin + part_rows], "sp", axis=0, tiled=True)
        scale = scales[:, begin : begin + part_rows].reshape(-1, 1)
        produced = run_experts(
            gathered, scale, exp_gate[0], exp_up[0], exp_down[0], side_w, side_down
        )
        sums.append(lax.psum_scatter(produced, "sp", scatter_dimension=0, tiled=True))
    added = jnp.concatenate(sums, axis=0)
    return (resid.astype(jnp.float32) + added.astype(jnp.float32)).astype(jnp.bfloat16)


def solution(mesh):
    placed = (
        P("sp", "tp"),
        P("sp", "tp"),
        P("sp", "tp"),
        P("sp"),
        P("tp"),
        P("tp", None),
        P(("sp", "tp"), None),
        P(),
        P(("sp", "tp"), None),
        P(("sp", "tp"), None),
        P("sp", None, None),
        P("sp", None, None),
        P("sp", None, None),
        P(None, "tp"),
        P(None, "tp"),
        P("tp", None),
    )
    return jax.shard_map(
        shards, mesh=mesh, in_specs=placed, out_specs=P(("sp", "tp"), None), check_vma=False
    )
```

profile of v0, /device:TPU:0, one launch (start us, length us, event | category | flops | bytes accessed | tf_op | source)
XLA Modules:
  0.0 454.8 jit_solution(13340162137230098640)
XLA Ops:
  7.5 1.5 pad_maximum_fusion.6
  9.1 3.0 collective-permute-start
  13.4 2.2 reshape.84
  21.0 1.6 copy.102
  22.5 1.6 copy.103
  24.1 1.6 copy.104
  28.3 1.8 fusion.1
  30.2 1.8 fusion
  34.1 5.7 %fusion.10 = bf16[2,256,2,4,64]{1,4,3,2,0:T(8,128)(2,1)S(1)} fusion(bf16[2,512,2,64,1]{1,3,4,2,0:T(8,128)(2,1)S(1)} %bitcast.63, f32[2,2,512,256,4]{3,2,4,1,0:T(8,128)} %copy-done.4, f32[2,2,4,256]{3,2,1,0:T(4,128)S(1)} %exponential_add_fusion, f32[2,2,4,256]{3,2,1,0:T(4,128)S(1)} %broadcast_maximum_fusion, pred[2,256,512]{1,2,0:T(8,128)(4,1)S(1)} %compare_and_fusion), kind=kOutput, calls=%fused_computation.20 | convolution fusion | flops 279183360 | bytes 9469952 | tf_op jit(solution)/shard_map/nkgqm,nmkd->nqkgd/dot_general | solution.py:79
  40.4 2.6 convolution_convert_fusion
  43.1 36.0 %reduce-scatter.4.cloned.1.call-done = bf16[256,2048]{1,0:T(8,128)(2,1)} async-done(((bf16[512,2048]{1,0:T(8,128)(2,1)}), bf16[256,2048]{1,0:T(8,128)(2,1)}) %reduce-scatter.4.cloned.1.call-update) | async-done | bytes 1048592 | tf_op jit(solution)/shard_map/reduce_scatter | solution.py:187
  79.1 1.7 fusion.3
  83.2 1.4 constant_dynamic-slice_fusion.1
  87.0 5.8 %all-to-all-start = ((f32[16,1,256]{2,1,0:T(1,128)}), f32[16,1,256]{2,1,0:T(1,128)S(1)}, u32[]{:S(2)}, u32[]{:S(2)}) async-start(f32[16,1,256]{2,1,0:T(1,128)} %copy.85), calls=%async_computation.1 | async-start | bytes 32768 | tf_op jit(solution)/shard_map/all_to_all | solution.py:204
  93.1 6.6 %all-to-all-done = f32[16,1,256]{2,1,0:T(1,128)S(1)} async-done(((f32[16,1,256]{2,1,0:T(1,128)}), f32[16,1,256]{2,1,0:T(1,128)S(1)}, u32[]{:S(2)}, u32[]{:S(2)}) %all-to-all-start) | async-done | bytes 16416 | tf_op jit(solution)/shard_map/all_to_all | solution.py:204
  101.0 56.2 %all-gather.3.cloned.1.call-done.rows_ref = bf16[2048,2048]{1,0:T(8,128)(2,1)} async-done(((bf16[128,2048]{1,0:T(8,128)(2,1)}), bf16[2048,2048]{1,0:T(8,128)(2,1)}) %all-gather.3.cloned.1.call-update) | async-done | bytes 8388624 | tf_op jit(solution)/shard_map/all_gather | solution.py:209
  157.2 1.6 copy-done.2
  158.8 28.0 %shard_map.154 = bf16[2048,2048]{1,0:T(8,128)(2,1)} custom-call(bf16[2048,2048]{1,0:T(8,128)(2,1)} %all-gather.3.cloned.1.call-done.rows_ref, f32[2048,1]{1,0:T(8,128)S(1)} %copy.88.scale_ref, bf16[2048,512]{1,0:T(8,128)(2,1)S(1)} %bitcast.52, bf16[2048,512]{1,0:T(8,128)(2,1)} %bitcast.72, bf16[512,2048]{1,0:T(8,128)(2,1)} %bitcast.74, ...), custom_call_target="tpu_custom_call" | custom-call | flops 16106127360 | bytes 24641536 | tf_op jit(solution)/shard_map/pallas_call | solution.py:106
  187.2 45.0 %all-gather.5.cloned.1.call-done.rows_ref = bf16[2048,2048]{1,0:T(8,128)(2,1)} async-done(((bf16[128,2048]{1,0:T(8,128)(2,1)}), bf16[2048,2048]{1,0:T(8,128)(2,1)}) %all-gather.5.cloned.1.call-update) | async-done | bytes 8388624 | tf_op jit(solution)/shard_map/all_gather | solution.py:209
  232.3 1.6 copy-done.3
  233.8 28.1 %shard_map.155 = bf16[2048,2048]{1,0:T(8,128)(2,1)} custom-call(bf16[2048,2048]{1,0:T(8,128)(2,1)} %all-gather.5.cloned.1.call-done.rows_ref, f32[2048,1]{1,0:T(8,128)S(1)} %copy.90.scale_ref, bf16[2048,512]{1,0:T(8,128)(2,1)S(1)} %bitcast.53, bf16[2048,512]{1,0:T(8,128)(2,1)} %bitcast.73, bf16[512,2048]{1,0:T(8,128)(2,1)} %bitcast.75, ...), custom_call_target="tpu_custom_call" | custom-call | flops 16106127360 | bytes 24641536 | tf_op jit(solution)/shard_map/pallas_call | solution.py:106
  262.0 76.3 %reduce-scatter.6.cloned.1.call-done = bf16[128,2048]{1,0:T(8,128)(2,1)} async-done(((bf16[2048,2048]{1,0:T(8,128)(2,1)}), bf16[128,2048]{1,0:T(8,128)(2,1)}) %reduce-scatter.6.cloned.1.call-update) | async-done | bytes 524304 | tf_op jit(solution)/shard_map/reduce_scatter | solution.py:214
  338.2 107.0 %reduce-scatter.8.cloned.1.call-done = bf16[128,2048]{1,0:T(8,128)(2,1)} async-done(((bf16[2048,2048]{1,0:T(8,128)(2,1)}), bf16[128,2048]{1,0:T(8,128)(2,1)}) %reduce-scatter.8.cloned.1.call-update) | async-done | bytes 524304 | tf_op jit(solution)/shard_map/reduce_scatter | solution.py:214
  445.2 3.1 fusion.6
  (88 shorter events, 19.7 us)
Async XLA Ops:
  6.5 33.8 %copy-start = (bf16[512,2048]{1,0:T(8,128)(2,1)S(1)}, bf16[512,2048]{1,0:T(8,128)(2,1)}, u32[]{:S(2)}) copy-start(bf16[512,2048]{1,0:T(8,128)(2,1)} %param.21) | copy-start | bytes 6291460
  6.5 10.6 %copy-start.9 = (bf16[512,128]{1,0:T(8,128)(2,1)S(1)}, bf16[512,128]{1,0:T(8,128)(2,1)}, u32[]{:S(2)}) copy-start(bf16[512,128]{1,0:T(8,128)(2,1)} %param.18) | copy-start | bytes 393220
  6.5 9.1 %copy-start.14 = (f32[8]{0:T(128)S(1)}, f32[8]{0:T(128)}, u32[]{:S(2)}) copy-start(f32[8]{0:T(128)} %param.20) | copy-start | bytes 100
  6.5 72.5 %reduce-scatter.4.cloned.1.call-start = ((), (), s32[]{:S(2)}) async-start(), calls=%async_computation.4 | async-start | bytes 3145728 | tf_op jit(solution)/shard_map/reduce_scatter | solution.py:187
  9.1 6.8 %collective-permute-start = (bf16[128,384]{1,0:T(8,128)(2,1)}, bf16[128,384]{1,0:T(8,128)(2,1)}, u32[]{:S(2)}, u32[]{:S(2)}) collective-permute-start(bf16[128,384]{1,0:T(8,128)(2,1)} %get-tuple-element.12), channel_id=1, source_target_pairs={{0,2},{2,4},{4,6},{6,8},{8,10},{10,12},{12,14},{14,16},{16,18},{18... | collective-permute-start | bytes 294920 | tf_op jit(solution)/shard_map/ppermute | solution.py:26
  12.1 5.0 %collective-permute-start.1 = (bf16[128,384]{1,0:T(8,128)(2,1)}, bf16[128,384]{1,0:T(8,128)(2,1)}, u32[]{:S(2)}, u32[]{:S(2)}) collective-permute-start(bf16[128,384]{1,0:T(8,128)(2,1)} %get-tuple-element.13), channel_id=1, source_target_pairs={{2,0},{4,2},{6,4},{8,6},{10,8},{12,10},{14,12},{16,14},{18,16},{20... | collective-permute-start | bytes 294920 | tf_op jit(solution)/shard_map/ppermute | solution.py:28
  30.1 3.2 copy-start.4
  30.2 3.2 copy-start.8
  43.0 36.1 %copy-start.5 = (bf16[256,2048]{1,0:T(8,128)(2,1)S(1)}, bf16[256,2048]{1,0:T(8,128)(2,1)}, u32[]{:S(2)}) copy-start(bf16[256,2048]{1,0:T(8,128)(2,1)} %param.22) | copy-start | bytes 3145732
  43.0 37.8 %copy-start.11 = (f32[2048]{0:T(1024)S(1)}, f32[2048]{0:T(1024)}, u32[]{:S(2)}) copy-start(f32[2048]{0:T(1024)} %param.23) | copy-start | bytes 24580
  43.0 114.1 %all-gather.3.cloned.1.call-start = ((), (), s32[]{:S(2)}) async-start(), calls=%async_computation.5 | async-start | bytes 8912896 | tf_op jit(solution)/shard_map/all_gather | solution.py:209
  79.1 1.8 copy-start.7
  81.3 1.9 copy-start.10
  82.4 149.8 %all-gather.5.cloned.1.call-start = ((), (), s32[]{:S(2)}) async-start(), calls=%async_computation.7 | async-start | bytes 8912896 | tf_op jit(solution)/shard_map/all_gather | solution.py:209
  83.2 3.2 copy-start.12
  83.2 3.2 copy-start.13
  86.0 14.2 %collective-permute-start.2 = (bf16[96,2048]{1,0:T(8,128)(2,1)S(1)}, bf16[96,2048]{1,0:T(8,128)(2,1)S(1)}, u32[]{:S(2)}, u32[]{:S(2)}) collective-permute-start(bf16[96,2048]{1,0:T(8,128)(2,1)S(1)} %pad_maximum_fusion.1), channel_id=1, source_target_pairs={{0,1},{1,0},{2,3},{3,2},{4,5},{5,4},{6,7},{7,6},{8,9},{9,8},{10,11... | collective-permute-start | bytes 1179656 | tf_op jit(solution)/shard_map/ppermute | solution.py:147
  87.0 12.7 %all-to-all-start = ((f32[16,1,256]{2,1,0:T(1,128)}), f32[16,1,256]{2,1,0:T(1,128)S(1)}, u32[]{:S(2)}, u32[]{:S(2)}) async-start(f32[16,1,256]{2,1,0:T(1,128)} %copy.85), calls=%async_computation.1 | async-start | bytes 32768 | tf_op jit(solution)/shard_map/all_to_all | solution.py:204
  92.9 245.4 %reduce-scatter.6.cloned.1.call-start = ((), (), s32[]{:S(2)}) async-start(), calls=%async_computation.6 | async-start | bytes 8912896 | tf_op jit(solution)/shard_map/reduce_scatter | solution.py:214
  157.2 1.6 copy-start.2
  186.8 258.4 %reduce-scatter.8.cloned.1.call-start = ((), (), s32[]{:S(2)}) async-start(), calls=%async_computation.8 | async-start | bytes 8912896 | tf_op jit(solution)/shard_map/reduce_scatter | solution.py:214
  232.3 1.6 copy-start.3
  261.9 183.3 %copy-start.6 = (bf16[256,2048]{1,0:T(8,128)(2,1)S(1)}, bf16[256,2048]{1,0:T(8,128)(2,1)}, u32[]{:S(2)}) copy-start(bf16[256,2048]{1,0:T(8,128)(2,1)} %param.22) | copy-start | bytes 3145732
  261.9 186.3 %copy-start.1 = (bf16[512,2048]{1,0:T(8,128)(2,1)S(1)}, bf16[512,2048]{1,0:T(8,128)(2,1)}, u32[]{:S(2)}) copy-start(bf16[512,2048]{1,0:T(8,128)(2,1)} %param.21) | copy-start | bytes 6291460
Sparse Core Ops, SparseCore 0:
  43.1 35.8 reduce-scatter.3
  82.5 74.5 all-gather.2
  159.3 72.8 all-gather.4
  236.2 102.0 reduce-scatter.5
  342.1 103.0 reduce-scatter.7
where the time goes:
time: 455 us
  waiting for transfers between devices  329 us (72%)
  Pallas kernels  56.1 us (12%)
  local copies, waits for them, and re-layouts  22.1 us (5%)
  between operations  13.5 us (3%)
  other arithmetic  12.9 us (3%)
  starting transfers between devices  10.9 us (2%)
  matrix products  10.1 us (2%)
    reduce_scatter x2, waiting for transfers between devices, shards(): lax.psum_scatter(produced, 'sp', scatter_dimension=0, tiled=True)  183 us
    all_gather x2, waiting for transfers between devices, shards(): lax.all_gather(normed[begin:begin + part_rows], 'sp', axis=0, tiled=True)  101 us
    pallas_call x2, Pallas kernels, run_experts(): pl.pallas_call(expert_kernel, grid=(count // tile,), in_specs=[pl.BlockSp...  56.1 us
    reduce_scatter x1, waiting for transfers between devices, shards(): lax.psum_scatter(jnp.dot(attended, w_out, preferred_element_type=jnp.floa...  36 us
    unnamed x42, local copies, waits for them, and re-layouts  11 us
  transfers between devices with their start and end apart: 9, of which 7 were waited for; matrix products, arithmetic and copies ran while one was open for 2% of the time, Pallas kernels for 12%

commit v1 on v0

--- a/solution.py
+++ b/solution.py
@@ -216,7 +216,575 @@
     return (resid.astype(jnp.float32) + added.astype(jnp.float32)).astype(jnp.bfloat16)
 
 
+MESH = pl.DeviceIdType.MESH
+QB = 128
+NEG = -1e30
+LINE = 4
+
+
+def layer_kernel(
+    tab_in, marks_in, sink_ref, q_in, k_in, v_in, wo_in, res_in, gain_ref,
+    eg_in, eu_in, ed_in, sg_in, su_in, sd_in,
+    out_ref,
+    q_s, kx, vx, marks, kk, vv, a_out, a_own, a_in, wo_own, wo_oth, res, tok, tab, tabt,
+    gs, us, ds, hid, acc, stage, rbuf, sg, su, sd, sh, ost,
+    loc, halo_s, halo_r, tab_s, tab_r, wo_s, wo_r, att_s, att_r,
+    sib_s, sib_r, y_s, y_r, x_s, x_r, fy_s, fy_r, fx_s, fx_r,
+    ag_s, ag_r, rs_s, rs_r, sx_s, sx_r, ss_s, ss_r, out_sem,
+):
+    f32, bf16 = jnp.float32, jnp.bfloat16
+    sp_count, tp_count = lax.axis_size("sp"), lax.axis_size("tp")
+    s, x = lax.axis_index("sp"), lax.axis_index("tp")
+    z, y, c = s // 4, lax.rem(s // 2, 2), lax.rem(s, 2)
+    ox, oy, oc = 1 - x, 1 - y, 1 - c
+    at = lambda zz, yy, cc: (zz * 2 + yy) * 2 + cc
+    dev = lambda sp, tp: {"sp": sp, "tp": tp}
+    sib, ypar, xpar = dev(at(z, y, oc), x), dev(at(z, oy, c), x), dev(s, ox)
+    nxt, prv = dev(lax.rem(s + 1, sp_count), x), dev(lax.rem(s + sp_count - 1, sp_count), x)
+    low = z < 2
+    w = jnp.where(low, z, 3 - z)
+    inner = w == 1
+    zf = jnp.where(low, z + 1, z - 1)
+    zb = jnp.clip(jnp.where(low, z - 1, z + 1), 0, 3)
+    fwd, bck = dev(at(zf, y, c), x), dev(at(zb, y, c), x)
+    line = lambda ob: jnp.where(low, ob, 3 - ob)
+    tokens = q_in.shape[0]
+    half = tokens // 2
+    width = res_in.shape[1]
+    ff = eg_in.shape[2]
+    part = width // 4
+
+    def send(src, dst, ss, rs, to):
+        cp = pltpu.make_async_remote_copy(
+            src_ref=src, dst_ref=dst, send_sem=ss, recv_sem=rs, device_id=to, device_id_type=MESH
+        )
+        cp.start()
+        return cp
+
+    def got(view, rs):
+        pltpu.make_async_remote_copy(
+            src_ref=view, dst_ref=view, send_sem=rs, recv_sem=rs, device_id=sib, device_id_type=MESH
+        ).wait_recv()
+
+    def sent(view, ss):
+        pltpu.make_async_remote_copy(
+            src_ref=view, dst_ref=view, send_sem=ss, recv_sem=ss, device_id=sib, device_id_type=MESH
+        ).wait_send()
+
+    def load(src, dst, sem):
+        cp = pltpu.make_async_copy(src, dst, sem)
+        cp.start()
+        return cp
+
+    rows_own = pl.ds(QB, tokens)
+    loads_a = [
+        load(q_in, q_s, loc.at[0]),
+        load(k_in, kx.at[rows_own], loc.at[1]),
+        load(v_in, vx.at[rows_own], loc.at[2]),
+        load(marks_in, marks.at[pl.ds(1, tokens // QB)], loc.at[3]),
+    ]
+    loads_b = [
+        load(wo_in, wo_own, loc.at[4]),
+        load(res_in, res, loc.at[5]),
+        load(tab_in, tab.at[z], loc.at[6]),
+        load(eg_in.at[0], gs.at[0], loc.at[7]),
+        load(eu_in.at[0], us.at[0], loc.at[8]),
+        load(sg_in, sg.at[0], loc.at[9]),
+        load(su_in, su.at[0], loc.at[10]),
+        load(sd_in, sd.at[pl.ds(0, sd_in.shape[0])], loc.at[11]),
+    ]
+    for n in range(4):
+        loads_b.append(
+            load(ed_in.at[0, :, pl.ds(n * part, part)], ds.at[n, pl.ds(0, ff)], loc.at[12 + n])
+        )
+
+    barrier = pltpu.get_barrier_semaphore()
+    zs = [lax.rem(z + i, LINE) for i in range(1, LINE)]
+    partners = [nxt, prv, sib, ypar, xpar] + [dev(at(zz, y, c), x) for zz in zs]
+    for to in partners:
+        pl.semaphore_signal(barrier, inc=1, device_id=to, device_id_type=MESH)
+    pl.semaphore_wait(barrier, len(partners))
+
+    pend = []
+    last, first = pl.ds(tokens - QB, QB), pl.ds(0, QB)
+    after = pl.ds(QB + tokens, QB)
+    nb = tokens // QB
+    for i, (src, dst, lo, hi, a, b) in enumerate(
+        [(k_in, kx, first, after, last, first), (v_in, vx, first, after, last, first)]
+    ):
+        pend.append(send(src.at[a], dst.at[lo], halo_s.at[2 * i], halo_r.at[2 * i], nxt))
+        pend.append(send(src.at[b], dst.at[hi], halo_s.at[2 * i + 1], halo_r.at[2 * i + 1], prv))
+    pend.append(send(marks_in.at[nb - 1], marks.at[0], halo_s.at[4], halo_r.at[4], nxt))
+    pend.append(send(marks_in.at[0], marks.at[nb + 1], halo_s.at[5], halo_r.at[5], prv))
+    for i, zz in enumerate(zs):
+        pend.append(send(tab_in, tab.at[z], tab_s.at[i], tab_r.at[LINE - 2 - i], dev(at(zz, y, c), x)))
+
+    wrows = wo_in.shape[0] // 2
+    wmine, woth = pl.ds(c * wrows, wrows), pl.ds(oc * wrows, wrows)
+    pend.append(send(wo_in.at[wmine], wo_oth.at[wmine], wo_s.at[0], wo_r.at[0], xpar))
+
+    quarter = width // 4
+
+    def piece(refs, kind, i, slot):
+        g, u, d = refs
+        if kind == "g":
+            return g.at[slot, pl.ds(i * quarter, quarter)]
+        if kind == "u":
+            return u.at[slot, pl.ds(i * quarter, quarter)]
+        if slot is None:
+            return d.at[0, :, pl.ds(i * part, part)]
+        return d.at[i, pl.ds(slot * ff, ff)]
+
+    def hbm_piece(kind, i):
+        if kind == "g":
+            return eg_in.at[0, pl.ds(i * quarter, quarter)]
+        if kind == "u":
+            return eu_in.at[0, pl.ds(i * quarter, quarter)]
+        return ed_in.at[0, :, pl.ds(pl.multiple_of(i * part, part), part)]
+
+    held = (gs, us, ds)
+    own_only = lambda v: [("g", 2 * v), ("g", 2 * v + 1), ("u", v), ("d", v), ("d", 2 + v)]
+    y_list = own_only(x)[:3] + [("u", 2), ("u", 3)] + own_only(x)[3:]
+    x_list = own_only(ox)
+    y_to_x = {0: 0, 1: 1, 2: 2, 5: 3, 6: 4}
+    for i, (kind, j) in enumerate(y_list):
+        pend.append(send(hbm_piece(kind, j), piece(held, kind, j, 2), y_s.at[i], y_r.at[i], ypar))
+    pend.append(send(eg_in.at[0], gs.at[1], sib_s.at[0], sib_r.at[0], sib))
+    pend.append(send(eu_in.at[0], us.at[1], sib_s.at[1], sib_r.at[1], sib))
+    for n in range(4):
+        pend.append(
+            send(hbm_piece("d", n), piece(held, "d", n, 1), sib_s.at[2 + n], sib_r.at[2 + n], sib)
+        )
+
+    def y_event(i):
+        kind, j = y_list[i]
+        view = piece(held, kind, j, 2)
+        got(view, y_r.at[i])
+        if i in y_to_x:
+            pend.append(send(view, view, x_s.at[y_to_x[i]], x_r.at[y_to_x[i]], xpar))
+        pend.append(send(view, piece(held, kind, j, 3), fy_s.at[i], fy_r.at[i], sib))
+
+    def x_event(i):
+        kind, j = x_list[i]
+        view = piece(held, kind, j, 2)
+        got(view, x_r.at[i])
+        pend.append(send(view, piece(held, kind, j, 3), fx_s.at[i], fx_r.at[i], sib))
+
+    for cp in loads_a:
+        cp.wait()
+    for i in range(2):
+        dst = (kx, vx)[i]
+        got(dst.at[first], halo_r.at[2 * i])
+        got(dst.at[after], halo_r.at[2 * i + 1])
+    got(marks.at[0], halo_r.at[4])
+    got(marks.at[nb + 1], halo_r.at[5])
+
+    @pl.when(s == 0)
+    def _():
+        marks[0] = jnp.full(marks.shape[1:], -1, jnp.int32)
+
+    @pl.when(s == sp_count - 1)
+    def _():
+        marks[nb + 1] = jnp.full(marks.shape[1:], -1, jnp.int32)
+
+    ri = lax.broadcasted_iota(jnp.int32, (QB, QB), 0)
+    ci = lax.broadcasted_iota(jnp.int32, (QB, QB), 1)
+    swap = jnp.where(ci == lax.rem(ri + HD, QB), 1.0, 0.0).astype(bf16)
+
+    def spread(t, carry):
+        rows = pl.ds(pl.multiple_of(t * QB, QB), QB)
+        for src, dst in ((kx, kk), (vx, vv)):
+            cur = src[rows]
+            turned = jnp.dot(cur, swap, preferred_element_type=f32)
+            cur = cur.astype(f32)
+            zero = jnp.zeros_like(cur)
+            left = ci < HD
+            dst[0, rows] = jnp.where(left, cur, zero).astype(bf16)
+            dst[1, rows] = jnp.where(left, zero, turned).astype(bf16)
+            dst[2, rows] = jnp.where(left, turned, zero).astype(bf16)
+            dst[3, rows] = jnp.where(left, zero, cur).astype(bf16)
+        return carry
+
+    lax.fori_loop(0, nb + 2, spread, 0)
+
+    def attend_rows(blk, dst, drow):
+        rows = pl.ds(pl.multiple_of(blk * QB, QB), QB)
+        span = pl.ds(pl.multiple_of(blk * QB, QB), 3 * QB)
+        mine = jnp.broadcast_to(marks[blk + 1][0:1], (QB, QB)).T
+        biases = []
+        for t in range(3):
+            same = mine == jnp.broadcast_to(marks[blk + t][0:1], (QB, QB))
+            if t == 0:
+                same = same & (ri <= ci)
+            if t == 2:
+                same = same & (ci <= ri)
+            biases.append(jnp.where(same, 0.0, NEG).astype(f32))
+        bias = jnp.concatenate(biases, axis=1)
+        for j in range(q_s.shape[1] // QB):
+            g = j // 2
+            keys2 = jnp.concatenate([kk[2 * g, span], kk[2 * g + 1, span]], axis=0)
+            vals2 = jnp.concatenate([vv[2 * g, span], vv[2 * g + 1, span]], axis=0)
+            sc = lax.dot_general(
+                q_s[rows, j * QB : (j + 1) * QB], keys2, (((1,), (1,)), ((), ())),
+                preferred_element_type=f32,
+            ) * HD ** (-0.5)
+            probs = []
+            for h in range(2):
+                sink = sink_ref[2 * j + h]
+                own = sc[:, h * 3 * QB : (h + 1) * 3 * QB] + bias
+                top = jnp.maximum(jnp.max(own, axis=-1, keepdims=True), sink)
+                e = jnp.exp(own - top)
+                total = jnp.sum(e, axis=-1, keepdims=True) + jnp.exp(sink - top)
+                probs.append((e * (1.0 / total)).astype(bf16))
+            o = jnp.dot(jnp.concatenate(probs, axis=1), vals2, preferred_element_type=f32)
+            dst[pl.ds(pl.multiple_of(drow, QB), QB), j * QB : (j + 1) * QB] = o.astype(bf16)
+
+    hb = half // QB
+
+    def other_rows(i, carry):
+        attend_rows(ox * hb + i, a_out, i * QB)
+        piece_rows = pl.ds(pl.multiple_of(i * QB, QB), QB)
+        send(a_out.at[piece_rows], a_in.at[piece_rows], att_s.at[i], att_r.at[i], xpar)
+        return carry
+
+    lax.fori_loop(0, hb, other_rows, 0)
+
+    def own_rows(i, carry):
+        attend_rows(x * hb + i, a_own, i * QB)
+        return carry
+
+    lax.fori_loop(0, hb, own_rows, 0)
+
+    for cp in loads_b:
+        cp.wait()
+    y_event(0)
+    got(wo_oth.at[wmine], wo_r.at[0])
+    pend.append(send(wo_oth.at[wmine], wo_oth.at[wmine], wo_s.at[1], wo_r.at[1], sib))
+    for i in range(hb):
+        got(a_in.at[pl.ds(i * QB, QB)], att_r.at[i])
+    got(wo_oth.at[woth], wo_r.at[1])
+    square = jnp.zeros((half, 1), f32)
+    for n in range(4):
+        cols = slice(n * part, (n + 1) * part)
+        mixed = jnp.dot(a_own[...], wo_own[:, cols], preferred_element_type=f32)
+        mixed = mixed + jnp.dot(a_in[...], wo_oth[:, cols], preferred_element_type=f32)
+        r = (res[:, cols].astype(f32) + mixed).astype(bf16)
+        res[:, cols] = r
+        rf = r.astype(f32)
+        square = square + jnp.sum(rf * rf, axis=-1, keepdims=True)
+    inv = lax.rsqrt(square * (1.0 / width) + norm_eps)
+    for n in range(4):
+        cols = slice(n * part, (n + 1) * part)
+        tok[z, :, cols] = (res[:, cols].astype(f32) * inv * gain_ref[:, cols]).astype(bf16)
+
+    hr = half // 2
+    rows_of = lambda r: pl.ds(r * hr, hr)
+
+    def ag_send(b, r, direction, to):
+        view = tok.at[b, rows_of(r)]
+        send(view, view, ag_s.at[direction, b, r], ag_r.at[b, r], to)
+
+    def ag_sent(b, r, direction):
+        sent(tok.at[b, rows_of(r)], ag_s.at[direction, b, r])
+
+    def ag_got(b, r):
+        got(tok.at[b, rows_of(r)], ag_r.at[b, r])
+
+    for r in range(2):
+        ag_send(z, r, 0, fwd)
+
+        @pl.when(inner)
+        def _():
+            ag_send(z, r, 1, bck)
+
+    def relay(ob, r):
+        b = line(ob)
+
+        @pl.when(inner)
+        def _():
+            ag_got(b, r)
+            if ob == 0:
+                ag_send(b, r, 0, fwd)
+            else:
+                ag_send(b, r, 1, bck)
+
+    def table_columns(b, carry):
+        t = tab[b]
+        grown = jnp.concatenate([t, jnp.zeros((QB - t.shape[0], t.shape[1]), f32)], axis=0)
+        tabt[b] = grown.T
+        return carry
+
+    lanes = lax.broadcasted_iota(jnp.int32, (half, QB), 1)
+
+    def gated(rows, gate, up):
+        a = jnp.dot(rows, gate, preferred_element_type=f32)
+        b = jnp.dot(rows, up, preferred_element_type=f32)
+        return a / (1.0 + jnp.exp(-a)) * b
+
+    def hidden(b, lo, hi):
+        def one(slot, carry):
+            e = at(z, jnp.where(slot >= 2, oy, y), jnp.where(lax.rem(slot, 2) == 1, oc, c))
+            scale = jnp.sum(jnp.where(lanes == e, tabt[b], 0.0), axis=-1, keepdims=True)
+            for h in range(2):
+                cols = slice(h * (ff // 2), (h + 1) * (ff // 2))
+                v = gated(tok[b], gs[slot, :, cols], us[slot, :, cols]) * scale
+                to = pl.ds(pl.multiple_of(slot * ff + h * (ff // 2), ff // 2), ff // 2)
+                hid[b, :, to] = v.astype(bf16)
+            return carry
+
+        lax.fori_loop(lo, hi, one, 0)
+
+    y_event(1)
+    for i in range(LINE - 1):
+        got(tab.at[z], tab_r.at[i])
+    lax.fori_loop(0, LINE, table_columns, 0)
+    got(gs.at[1], sib_r.at[0])
+    got(us.at[1], sib_r.at[1])
+    hidden(z, 0, 2)
+    y_event(2)
+    relay(0, 0)
+    relay(2, 0)
+    x_event(0)
+    y_event(3)
+    relay(0, 1)
+    relay(2, 1)
+    x_event(1)
+    y_event(4)
+    near = line(1 - w)
+
+    @pl.when(w == 0)
+    def _():
+        ag_got(near, 0)
+        ag_got(near, 1)
+
+    hidden(near, 0, 2)
+    relay(3, 0)
+    x_event(2)
+    y_event(5)
+    relay(3, 1)
+    srow, drow = sg_in.shape[0] // 2, sd_in.shape[0] // 2
+    shared_views = lambda core: [
+        sg.at[1, pl.ds(core * srow, srow)],
+        su.at[1, pl.ds(core * srow, srow)],
+        sd.at[pl.ds(sd_in.shape[0] + core * drow, drow)],
+    ]
+    for g in (2, 3):
+        pass
+    far2 = line(2)
+
+    @pl.when(w == 0)
+    def _():
+        ag_got(far2, 0)
+        ag_got(far2, 1)
+
+    for i in range(5):
+        kind, j = y_list[i]
+        got(piece(held, kind, j, 3), fy_r.at[i])
+    for i in range(3):
+        kind, j = x_list[i]
+        got(piece(held, kind, j, 3), fx_r.at[i])
+    hidden(far2, 0, 4)
+    for n in range(4):
+        got(piece(held, "d", n, 1), sib_r.at[2 + n])
+    y_event(6)
+    for i, (src, dst) in enumerate(
+        zip(
+            [
+                sg_in.at[pl.ds(c * srow, srow)],
+                su_in.at[pl.ds(c * srow, srow)],
+                sd_in.at[pl.ds(c * drow, drow)],
+            ],
+            shared_views(c),
+        )
+    ):
+        pend.append(send(src, dst, sx_s.at[i], sx_r.at[i], xpar))
+
+    order = [x, 2 + x, ox, 2 + ox]
+    tile = lambda slot, n: rbuf.at[slot, n]
+
+    def down(b, n):
+        return jnp.dot(hid[b], ds[n], preferred_element_type=f32)
+
+    def reduce_piece(step, n):
+        b = jnp.where(step == 2, near, line(2 + step))
+        slot = jnp.where(step == 0, 3 * w, jnp.where(step == 1, 1 + w, 4 - w))
+        zt = jnp.where((step == 2) & inner, zb, zf)
+        acc[...] = down(b, n)
+
+        @pl.when(inner)
+        def _():
+            got(tile(step, n), rs_r.at[step, n])
+            acc[...] = acc[...] + rbuf[step, n].astype(f32)
+
+        stage[step, n] = acc[...].astype(bf16)
+        send(
+            stage.at[step, n], tile(slot, n), rs_s.at[step, n], rs_r.at[slot, n], dev(at(zt, y, c), x)
+        )
+
+    for k in range(4):
+        kind, j = (y_list[5], y_list[6], x_list[3], x_list[4])[k]
+        if k >= 2:
+            x_event(k + 1)
+        got(piece(held, kind, j, 3), (fy_r.at[5], fy_r.at[6], fx_r.at[3], fx_r.at[4])[k])
+        reduce_piece(0, order[k])
+
+    def nth(k):
+        base = jnp.where(k < 2, x, ox)
+        return base + 2 * lax.rem(k, 2)
+
+    far3 = line(3)
+
+    @pl.when(w == 0)
+    def _():
+        ag_got(far3, 0)
+        ag_got(far3, 1)
+
+    hidden(far3, 0, 4)
+
+    def step_b(k, carry):
+        reduce_piece(1, nth(k))
+        return carry
+
+    lax.fori_loop(0, 4, step_b, 0)
+    hidden(near, 2, 4)
+
+    def step_c(k, carry):
+        reduce_piece(2, nth(k))
+        return carry
+
+    lax.fori_loop(0, 4, step_c, 0)
+
+    hidden(z, 2, 4)
+    for i, view in enumerate(shared_views(c)):
+        got(view, sx_r.at[i])
+        pend.append(send(view, view, ss_s.at[i], ss_r.at[i], sib))
+    for i, view in enumerate(shared_views(oc)):
+        got(view, ss_r.at[i])
+    units = sg_in.shape[1]
+    for h in range(2):
+        sh[:, h * units : (h + 1) * units] = gated(tok[z], sg[h], su[h]).astype(bf16)
+
+    def final(k, carry):
+        n = nth(k)
+        cols = pl.ds(pl.multiple_of(n * part, part), part)
+        acc[...] = (
+            res[:, cols].astype(f32)
+            + down(z, n)
+            + jnp.dot(sh[...], sd[:, cols], preferred_element_type=f32)
+        )
+        got(tile(3, n), rs_r.at[3, n])
+        acc[...] = acc[...] + rbuf[3, n].astype(f32)
+
+        @pl.when(inner)
+        def _():
+            got(tile(4, n), rs_r.at[4, n])
+            acc[...] = acc[...] + rbuf[4, n].astype(f32)
+
+        ost[n] = acc[...].astype(bf16)
+        load(ost.at[n], out_ref.at[:, cols], out_sem.at[n])
+        return carry
+
+    lax.fori_loop(0, 4, final, 0)
+
+    for cp in pend:
+        cp.wait_send()
+    for i in range(hb):
+        sent(a_out.at[pl.ds(i * QB, QB)], att_s.at[i])
+    for r in range(2):
+        ag_sent(z, r, 0)
+
+        @pl.when(inner)
+        def _():
+            ag_sent(z, r, 1)
+            ag_sent(line(0), r, 0)
+            ag_sent(line(2), r, 1)
+            ag_sent(line(3), r, 1)
+
+    for step in range(3):
+        for n in range(4):
+            sent(stage.at[step, n], rs_s.at[step, n])
+    for n in range(4):
+        pltpu.make_async_copy(ost.at[n], out_ref.at[:, pl.ds(n * part, part)], out_sem.at[n]).wait()
+
+
+def fused_shards(
+    queries, keys, values, doc_ids, sink_logit, w_out, residual, ffn_gain, expert_ids,
+    expert_weight, exp_gate, exp_up, exp_down, shared_gate, shared_up, shared_down,
+):
+    bf16, f32 = jnp.bfloat16, jnp.float32
+    experts = lax.axis_size("sp")
+    chosen = expert_ids.T[:, None, :] == jnp.arange(experts, dtype=jnp.int32)[None, :, None]
+    table = jnp.sum(jnp.where(chosen, expert_weight.T[:, None, :], 0.0), axis=0)
+    tokens = queries.shape[0]
+    nb = tokens // QB
+    marks = jnp.broadcast_to(doc_ids.reshape(nb, 1, QB), (nb, 8, QB))
+    half, width = residual.shape
+    ff = exp_gate.shape[2]
+    part = width // 4
+    units = shared_gate.shape[1]
+    heads = queries.shape[1]
+    vm = pltpu.VMEM
+    dma = pltpu.SemaphoreType.DMA
+    anyspace = pl.BlockSpec(memory_space=pl.ANY)
+    scratch = [
+        vm((tokens, heads), bf16),
+        vm((tokens + 2 * QB, QB), bf16),
+        vm((tokens + 2 * QB, QB), bf16),
+        vm((nb + 2, 8, QB), jnp.int32),
+        vm((4, tokens + 2 * QB, QB), bf16),
+        vm((4, tokens + 2 * QB, QB), bf16),
+        vm((half, heads), bf16),
+        vm((half, heads), bf16),
+        vm((half, heads), bf16),
+        vm(w_out.shape, bf16),
+        vm(w_out.shape, bf16),
+        vm((half, width), bf16),
+        vm((LINE, half, width), bf16),
+        vm((LINE, experts, half), f32),
+        vm((LINE, half, QB), f32),
+        vm((4, width, ff), bf16),
+        vm((4, width, ff), bf16),
+        vm((4, 4 * ff, part), bf16),
+        vm((LINE, half, 4 * ff), bf16),
+        vm((half, part), f32),
+        vm((3, 4, half, part), bf16),
+        vm((5, 4, half, part), bf16),
+        vm((2, width, units), bf16),
+        vm((2, width, units), bf16),
+        vm((2 * units, width), bf16),
+        vm((half, 2 * units), bf16),
+        vm((4, half, part), bf16),
+        dma((16,)), dma((6,)), dma((6,)), dma((3,)), dma((3,)), dma((2,)), dma((2,)),
+        dma((2,)), dma((2,)),
+        dma((6,)), dma((6,)), dma((7,)), dma((7,)), dma((5,)), dma((5,)), dma((7,)), dma((7,)),
+        dma((5,)), dma((5,)),
+        dma((2, LINE, 2)), dma((LINE, 2)), dma((3, 4)), dma((5, 4)),
+        dma((3,)), dma((3,)), dma((3,)), dma((3,)), dma((4,)),
+    ]
+    rows = LINE * half
+    return pl.pallas_call(
+        layer_kernel,
+        out_shape=jax.ShapeDtypeStruct((half, width), bf16),
+        in_specs=[anyspace, anyspace, pl.BlockSpec(memory_space=pltpu.SMEM)]
+        + [anyspace] * 5
+        + [pl.BlockSpec(memory_space=pltpu.VMEM)]
+        + [anyspace] * 6,
+        out_specs=anyspace,
+        scratch_shapes=scratch,
+        compiler_params=pltpu.CompilerParams(
+            collective_id=0, has_side_effects=True, vmem_limit_bytes=63 * 1024 * 1024
+        ),
+        cost_estimate=pl.CostEstimate(
+            flops=24 * rows * width * ff, bytes_accessed=32 * width * ff, transcendentals=rows * ff
+        ),
+    )(
+        table, marks, sink_logit, queries, keys, values, w_out, residual, ffn_gain.reshape(1, -1),
+        exp_gate, exp_up, exp_down, shared_gate, shared_up, shared_down,
+    )
+
+
 def solution(mesh):
+    fits = mesh.shape["tp"] == 2 and mesh.shape["sp"] == 4 * LINE
     placed = (
         P("sp", "tp"),
         P("sp", "tp"),
@@ -236,5 +804,5 @@
         P("tp", None),
     )
     return jax.shard_map(
-        shards, mesh=mesh, in_specs=placed, out_specs=P(("sp", "tp"), None), check_vma=False
-    )
+        fused_shards if fits else shards, mesh=mesh, in_specs=placed, out_specs=P(("sp", "tp"), None), check_vma=False
+    )

time: 455 us -> 171 us (0.38)
  waiting for transfers between devices: 329 us -> 0 us
  Pallas kernels: 56.1 us -> 165 us
  local copies, waits for them, and re-layouts: 22.1 us -> 3.59 us
  between operations: 13.5 us -> 0.01 us
  other arithmetic: 12.9 us -> 1.34 us
  starting transfers between devices: 10.9 us -> 0 us
  matrix products: 10.1 us -> 0 us
    reduce_scatter x3 -> x0, waiting for transfers between devices: 219 us -> none  [the longest x2 183 us: shards(): lax.psum_scatter(produced, 'sp', scatter_dimension=0, tiled=True)]
    pallas_call x2 -> x1, Pallas kernels: 56.1 us -> 165 us  [fused_shards(): pl.pallas_call(layer_kernel, out_shape=jax.ShapeDtypeStruct((half, width)...]
    all_gather x2 -> x0, waiting for transfers between devices: 101 us -> none  [shards(): lax.all_gather(normed[begin:begin + part_rows], 'sp', axis=0, tiled=True)]
    dot_general x3 -> x0, matrix products: 10.1 us -> none  [the longest x1 5.67 us: attend(): jnp.einsum('nkgqm,nmkd->nqkgd', attn_probs, value_blocks, preferred_eleme...]
    unnamed x42 -> x1, local copies, waits for them, and re-layouts: 11 us -> 2.3 us
    all_to_all x1 -> x0, waiting for transfers between devices: 6.63 us -> none  [shards(): lax.all_to_all(table.T, 'sp', split_axis=0, concat_axis=0, tiled=True)]
    all_to_all x1 -> x0, starting transfers between devices: 5.81 us -> none  [shards(): lax.all_to_all(table.T, 'sp', split_axis=0, concat_axis=0, tiled=True)]
    ppermute x3 -> x0, starting transfers between devices: 4.74 us -> none  [the longest x1 3.03 us: extended(): lax.ppermute(tail, axis, [(i, (i + 1) % count) for i in range(ends)])]
  transfers between devices with their start and end apart: 9 -> 0, of which waited for: 7 -> 0; matrix products, arithmetic and copies ran while one was open for 2% -> 0% of each run, Pallas kernels for 12% -> 0%
where the time goes in v1:
time: 171 us; the launch traced here: 170 us
  Pallas kernels  165 us (96%)
  local copies, waits for them, and re-layouts  3.59 us (2%)
    pallas_call x1, Pallas kernels, fused_shards(): pl.pallas_call(layer_kernel, out_shape=jax.ShapeDtypeStruct((half, width)...  165 us

profile of v1, /device:TPU:0, one launch (start us, length us, event | category | flops | bytes accessed | tf_op | source)
XLA Modules:
  0.0 170.2 jit_solution(6534867925803860940)
XLA Ops:
  0.0 1.3 broadcast_in_dim.25.marks_in
  1.3 1.3 select_reduce_fusion.tab_in
  2.6 165.3 %shard_map.154 = bf16[256,2048]{1,0:T(8,128)(2,1)} custom-call(f32[16,256]{1,0:T(8,128)} %select_reduce_fusion.tab_in, s32[4,8,128]{2,1,0:T(8,128)} %broadcast_in_dim.25.marks_in, f32[8]{0:T(128)} %sink_ref.1, bf16[512,512]{1,0:T(8,128)(2,1)} %q_in.1, bf16[512,128]{1,0:T(8,128)(2,1)} %k_in.1, bf16[512,128]{1,0:T(8,128)(2,1)} %v_in.1, ...), custom_call_target="tpu_custom_call" | custom-call | flops 25769803776 | bytes 33554432 | tf_op jit(solution)/shard_map/pallas_call | solution.py:765
  167.9 2.3 %copy.18 = bf16[256,2048]{1,0:T(8,128)(2,1)} copy(bf16[256,2048]{1,0:T(8,128)(2,1)} %shard_map.154) | data formatting | bytes 2097152

commit v2 on v1

--- a/solution.py
+++ b/solution.py
@@ -223,12 +223,12 @@
 
 
 def layer_kernel(
-    tab_in, marks_in, sink_ref, q_in, k_in, v_in, wo_in, res_in, gain_ref,
+    ids_in, wts_in, marks_in, sink_ref, q_in, k_in, v_in, wo_in, res_in, gain_ref,
     eg_in, eu_in, ed_in, sg_in, su_in, sd_in,
     out_ref,
-    q_s, kx, vx, marks, kk, vv, a_out, a_own, a_in, wo_own, wo_oth, res, tok, tab, tabt,
-    gs, us, ds, hid, acc, stage, rbuf, sg, su, sd, sh, ost,
-    loc, halo_s, halo_r, tab_s, tab_r, wo_s, wo_r, att_s, att_r,
+    q_s, kx, vx, marks, kk, vv, a_out, a_own, a_in, wo_own, wo_oth, res, tok, ids, wts, tab, tabt,
+    gs, us, ds, hid, acc, base, stage, rbuf, sg, su, sd, sh, ost,
+    loc, halo_s, halo_r, tab_s, tab_r, wx_s, wx_r, wz_s, wz_r, wf_s, wf_r, wg_s, wg_r, att_s, att_r,
     sib_s, sib_r, y_s, y_r, x_s, x_r, fy_s, fy_r, fx_s, fx_r,
     ag_s, ag_r, rs_s, rs_r, sx_s, sx_r, ss_s, ss_r, out_sem,
 ):
@@ -282,11 +282,12 @@
         load(k_in, kx.at[rows_own], loc.at[1]),
         load(v_in, vx.at[rows_own], loc.at[2]),
         load(marks_in, marks.at[pl.ds(1, tokens // QB)], loc.at[3]),
+        load(ids_in, ids, loc.at[6]),
+        load(wts_in, wts, loc.at[16]),
     ]
     loads_b = [
         load(wo_in, wo_own, loc.at[4]),
         load(res_in, res, loc.at[5]),
-        load(tab_in, tab.at[z], loc.at[6]),
         load(eg_in.at[0], gs.at[0], loc.at[7]),
         load(eu_in.at[0], us.at[0], loc.at[8]),
         load(sg_in, sg.at[0], loc.at[9]),
@@ -316,12 +317,24 @@
         pend.append(send(src.at[b], dst.at[hi], halo_s.at[2 * i + 1], halo_r.at[2 * i + 1], prv))
     pend.append(send(marks_in.at[nb - 1], marks.at[0], halo_s.at[4], halo_r.at[4], nxt))
     pend.append(send(marks_in.at[0], marks.at[nb + 1], halo_s.at[5], halo_r.at[5], prv))
-    for i, zz in enumerate(zs):
-        pend.append(send(tab_in, tab.at[z], tab_s.at[i], tab_r.at[LINE - 2 - i], dev(at(zz, y, c), x)))
-
-    wrows = wo_in.shape[0] // 2
-    wmine, woth = pl.ds(c * wrows, wrows), pl.ds(oc * wrows, wrows)
-    pend.append(send(wo_in.at[wmine], wo_oth.at[wmine], wo_s.at[0], wo_r.at[0], xpar))
+
+    pair = dev(at(jnp.where(inner, zb, zf), y, c), x)
+    wrows = wo_in.shape[0] // 8
+    wpiece = lambda pos, core, i: pl.ds(pl.multiple_of(((pos * 2 + core) * 2 + i) * wrows, wrows), wrows)
+    for i in range(2):
+        rows = wpiece(w, c, i)
+        pend.append(send(wo_in.at[rows], wo_oth.at[rows], wx_s.at[i], wx_r.at[i], xpar))
+
+    def wx_event(i):
+        view = wo_oth.at[wpiece(w, c, i)]
+        got(view, wx_r.at[i])
+        pend.append(send(view, view, wz_s.at[i], wz_r.at[i], pair))
+        pend.append(send(view, view, wf_s.at[i], wf_r.at[i], sib))
+
+    def wz_event(i):
+        view = wo_oth.at[wpiece(1 - w, c, i)]
+        got(view, wz_r.at[i])
+        pend.append(send(view, view, wg_s.at[i], wg_r.at[i], sib))
 
     quarter = width // 4
 
@@ -343,10 +356,10 @@
         return ed_in.at[0, :, pl.ds(pl.multiple_of(i * part, part), part)]
 
     held = (gs, us, ds)
-    own_only = lambda v: [("g", 2 * v), ("g", 2 * v + 1), ("u", v), ("d", v), ("d", 2 + v)]
-    y_list = own_only(x)[:3] + [("u", 2), ("u", 3)] + own_only(x)[3:]
-    x_list = own_only(ox)
-    y_to_x = {0: 0, 1: 1, 2: 2, 5: 3, 6: 4}
+    own_only = lambda v: [
+        ("g", 2 * v), ("g", 2 * v + 1), ("u", 2 * v), ("u", 2 * v + 1), ("d", v), ("d", 2 + v)
+    ]
+    y_list, x_list = own_only(x), own_only(ox)
     for i, (kind, j) in enumerate(y_list):
         pend.append(send(hbm_piece(kind, j), piece(held, kind, j, 2), y_s.at[i], y_r.at[i], ypar))
     pend.append(send(eg_in.at[0], gs.at[1], sib_s.at[0], sib_r.at[0], sib))
@@ -360,8 +373,7 @@
         kind, j = y_list[i]
         view = piece(held, kind, j, 2)
         got(view, y_r.at[i])
-        if i in y_to_x:
-            pend.append(send(view, view, x_s.at[y_to_x[i]], x_r.at[y_to_x[i]], xpar))
+        pend.append(send(view, view, x_s.at[i], x_r.at[i], xpar))
         pend.append(send(view, piece(held, kind, j, 3), fy_s.at[i], fy_r.at[i], sib))
 
     def x_event(i):
@@ -372,6 +384,16 @@
 
     for cp in loads_a:
         cp.wait()
+    lanes = lax.broadcasted_iota(jnp.int32, (half, QB), 1)
+    table = jnp.zeros((half, QB), f32)
+    for k in range(ids.shape[1]):
+        table = table + jnp.where(lanes == ids[:, k : k + 1], wts[:, k : k + 1], 0.0)
+    tabt[z] = table
+    tab[z] = table.T[: tab.shape[1]]
+    for i, zz in enumerate(zs):
+        pend.append(
+            send(tab.at[z], tab.at[z], tab_s.at[i], tab_r.at[LINE - 2 - i], dev(at(zz, y, c), x))
+        )
     for i in range(2):
         dst = (kx, vx)[i]
         got(dst.at[first], halo_r.at[2 * i])
@@ -441,34 +463,37 @@
 
     hb = half // QB
 
-    def other_rows(i, carry):
+    for i in range(hb):
         attend_rows(ox * hb + i, a_out, i * QB)
-        piece_rows = pl.ds(pl.multiple_of(i * QB, QB), QB)
-        send(a_out.at[piece_rows], a_in.at[piece_rows], att_s.at[i], att_r.at[i], xpar)
-        return carry
-
-    lax.fori_loop(0, hb, other_rows, 0)
-
-    def own_rows(i, carry):
+        rows = pl.ds(i * QB, QB)
+        pend.append(send(a_out.at[rows], a_in.at[rows], att_s.at[i], att_r.at[i], xpar))
+        if i == 0:
+            wx_event(0)
+    for i in range(hb):
         attend_rows(x * hb + i, a_own, i * QB)
-        return carry
-
-    lax.fori_loop(0, hb, own_rows, 0)
-
+
+    wx_event(1)
+    y_event(0)
     for cp in loads_b:
         cp.wait()
-    y_event(0)
-    got(wo_oth.at[wmine], wo_r.at[0])
-    pend.append(send(wo_oth.at[wmine], wo_oth.at[wmine], wo_s.at[1], wo_r.at[1], sib))
+    for n in range(4):
+        cols = slice(n * part, (n + 1) * part)
+        base[n] = res[:, cols].astype(f32) + jnp.dot(
+            a_own[...], wo_own[:, cols], preferred_element_type=f32
+        )
+    wz_event(0)
     for i in range(hb):
         got(a_in.at[pl.ds(i * QB, QB)], att_r.at[i])
-    got(wo_oth.at[woth], wo_r.at[1])
+    wz_event(1)
+    for i in range(2):
+        got(wo_oth.at[wpiece(w, oc, i)], wf_r.at[i])
+        got(wo_oth.at[wpiece(1 - w, oc, i)], wg_r.at[i])
     square = jnp.zeros((half, 1), f32)
     for n in range(4):
         cols = slice(n * part, (n + 1) * part)
-        mixed = jnp.dot(a_own[...], wo_own[:, cols], preferred_element_type=f32)
-        mixed = mixed + jnp.dot(a_in[...], wo_oth[:, cols], preferred_element_type=f32)
-        r = (res[:, cols].astype(f32) + mixed).astype(bf16)
+        r = (
+            base[n] + jnp.dot(a_in[...], wo_oth[:, cols], preferred_element_type=f32)
+        ).astype(bf16)
         res[:, cols] = r
         rf = r.astype(f32)
         square = square + jnp.sum(rf * rf, axis=-1, keepdims=True)
@@ -508,13 +533,12 @@
             else:
                 ag_send(b, r, 1, bck)
 
-    def table_columns(b, carry):
+    def table_columns(i, carry):
+        b = lax.rem(z + i, LINE)
         t = tab[b]
         grown = jnp.concatenate([t, jnp.zeros((QB - t.shape[0], t.shape[1]), f32)], axis=0)
         tabt[b] = grown.T
         return carry
-
-    lanes = lax.broadcasted_iota(jnp.int32, (half, QB), 1)
 
     def gated(rows, gate, up):
         a = jnp.dot(rows, gate, preferred_element_type=f32)
@@ -537,67 +561,52 @@
     y_event(1)
     for i in range(LINE - 1):
         got(tab.at[z], tab_r.at[i])
-    lax.fori_loop(0, LINE, table_columns, 0)
+    lax.fori_loop(1, LINE, table_columns, 0)
     got(gs.at[1], sib_r.at[0])
     got(us.at[1], sib_r.at[1])
     hidden(z, 0, 2)
-    y_event(2)
     relay(0, 0)
     relay(2, 0)
     x_event(0)
-    y_event(3)
+    y_event(2)
+    x_event(1)
     relay(0, 1)
     relay(2, 1)
-    x_event(1)
+    y_event(3)
+    near, far2, far3 = line(1 - w), line(2), line(3)
+
+    def end_got(b):
+        @pl.when(w == 0)
+        def _():
+            ag_got(b, 0)
+            ag_got(b, 1)
+
+    end_got(near)
+    hidden(near, 0, 2)
+    x_event(2)
+    relay(3, 0)
     y_event(4)
-    near = line(1 - w)
-
-    @pl.when(w == 0)
-    def _():
-        ag_got(near, 0)
-        ag_got(near, 1)
-
-    hidden(near, 0, 2)
-    relay(3, 0)
-    x_event(2)
-    y_event(5)
+    x_event(3)
     relay(3, 1)
+    for i in range(4):
+        kind, j = y_list[i]
+        got(piece(held, kind, j, 3), fy_r.at[i])
+        kind, j = x_list[i]
+        got(piece(held, kind, j, 3), fx_r.at[i])
+    hidden(near, 2, 4)
+    for n in range(4):
+        got(piece(held, "d", n, 1), sib_r.at[2 + n])
     srow, drow = sg_in.shape[0] // 2, sd_in.shape[0] // 2
     shared_views = lambda core: [
         sg.at[1, pl.ds(core * srow, srow)],
         su.at[1, pl.ds(core * srow, srow)],
         sd.at[pl.ds(sd_in.shape[0] + core * drow, drow)],
     ]
-    for g in (2, 3):
-        pass
-    far2 = line(2)
-
-    @pl.when(w == 0)
-    def _():
-        ag_got(far2, 0)
-        ag_got(far2, 1)
-
-    for i in range(5):
-        kind, j = y_list[i]
-        got(piece(held, kind, j, 3), fy_r.at[i])
-    for i in range(3):
-        kind, j = x_list[i]
-        got(piece(held, kind, j, 3), fx_r.at[i])
-    hidden(far2, 0, 4)
-    for n in range(4):
-        got(piece(held, "d", n, 1), sib_r.at[2 + n])
-    y_event(6)
-    for i, (src, dst) in enumerate(
-        zip(
-            [
-                sg_in.at[pl.ds(c * srow, srow)],
-                su_in.at[pl.ds(c * srow, srow)],
-                sd_in.at[pl.ds(c * drow, drow)],
-            ],
-            shared_views(c),
-        )
-    ):
-        pend.append(send(src, dst, sx_s.at[i], sx_r.at[i], xpar))
+    shared_parts = [
+        sg_in.at[pl.ds(c * srow, srow)],
+        su_in.at[pl.ds(c * srow, srow)],
+        sd_in.at[pl.ds(c * drow, drow)],
+    ]
 
     order = [x, 2 + x, ox, 2 + ox]
     tile = lambda slot, n: rbuf.at[slot, n]
@@ -621,40 +630,57 @@
             stage.at[step, n], tile(slot, n), rs_s.at[step, n], rs_r.at[slot, n], dev(at(zt, y, c), x)
         )
 
-    for k in range(4):
-        kind, j = (y_list[5], y_list[6], x_list[3], x_list[4])[k]
-        if k >= 2:
-            x_event(k + 1)
-        got(piece(held, kind, j, 3), (fy_r.at[5], fy_r.at[6], fx_r.at[3], fx_r.at[4])[k])
-        reduce_piece(0, order[k])
-
     def nth(k):
-        base = jnp.where(k < 2, x, ox)
-        return base + 2 * lax.rem(k, 2)
-
-    far3 = line(3)
-
-    @pl.when(w == 0)
-    def _():
-        ag_got(far3, 0)
-        ag_got(far3, 1)
-
+        base_n = jnp.where(k < 2, x, ox)
+        return base_n + 2 * lax.rem(k, 2)
+
+    def down_got(k):
+        lst, sem = (y_list, fy_r) if k < 2 else (x_list, fx_r)
+        kind, j = lst[4 + k % 2]
+        got(piece(held, kind, j, 3), sem.at[4 + k % 2])
+
+    def near_early(k):
+        @pl.when(w == 0)
+        def _():
+            reduce_piece(2, order[k])
+
+    down_got(0)
+    near_early(0)
+    end_got(far2)
+    hidden(far2, 0, 4)
+    y_event(5)
+    for i, (src, dst) in enumerate(zip(shared_parts, shared_views(c))):
+        pend.append(send(src, dst, sx_s.at[i], sx_r.at[i], xpar))
+    down_got(1)
+    near_early(1)
+    reduce_piece(0, order[0])
+    reduce_piece(0, order[1])
+    x_event(4)
+    down_got(2)
+    reduce_piece(0, order[2])
+    hidden(z, 2, 4)
+    x_event(5)
+    down_got(3)
+    reduce_piece(0, order[3])
+    end_got(far3)
     hidden(far3, 0, 4)
 
-    def step_b(k, carry):
-        reduce_piece(1, nth(k))
+    def later(i, carry):
+        even = lax.rem(i, 2) == 0
+        step = jnp.where(inner, jnp.where(even, 1, 2), jnp.where(i < 4, 1, 2))
+        k = jnp.where(inner, i // 2, jnp.where(i < 4, i, i - 2))
+        reduce_piece(step, nth(k))
         return carry
 
-    lax.fori_loop(0, 4, step_b, 0)
-    hidden(near, 2, 4)
-
-    def step_c(k, carry):
-        reduce_piece(2, nth(k))
+    def own_sum(n, carry):
+        cols = pl.ds(pl.multiple_of(n * part, part), part)
+        base[n] = res[:, cols].astype(f32) + down(z, n)
         return carry
 
-    lax.fori_loop(0, 4, step_c, 0)
-
-    hidden(z, 2, 4)
+    lax.fori_loop(0, 2, later, 0)
+    lax.fori_loop(0, 4, own_sum, 0)
+    lax.fori_loop(2, 6, later, 0)
+
     for i, view in enumerate(shared_views(c)):
         got(view, sx_r.at[i])
         pend.append(send(view, view, ss_s.at[i], ss_r.at[i], sib))
@@ -664,16 +690,19 @@
     for h in range(2):
         sh[:, h * units : (h + 1) * units] = gated(tok[z], sg[h], su[h]).astype(bf16)
 
+    def shared_sum(n, carry):
+        cols = pl.ds(pl.multiple_of(n * part, part), part)
+        base[n] = base[n] + jnp.dot(sh[...], sd[:, cols], preferred_element_type=f32)
+        return carry
+
+    lax.fori_loop(0, 4, shared_sum, 0)
+    lax.fori_loop(6, 6 + 2 * w, later, 0)
+
     def final(k, carry):
         n = nth(k)
         cols = pl.ds(pl.multiple_of(n * part, part), part)
-        acc[...] = (
-            res[:, cols].astype(f32)
-            + down(z, n)
-            + jnp.dot(sh[...], sd[:, cols], preferred_element_type=f32)
-        )
         got(tile(3, n), rs_r.at[3, n])
-        acc[...] = acc[...] + rbuf[3, n].astype(f32)
+        acc[...] = base[n] + rbuf[3, n].astype(f32)
 
         @pl.when(inner)
         def _():
@@ -688,8 +717,6 @@
 
     for cp in pend:
         cp.wait_send()
-    for i in range(hb):
-        sent(a_out.at[pl.ds(i * QB, QB)], att_s.at[i])
     for r in range(2):
         ag_sent(z, r, 0)
 
@@ -713,11 +740,9 @@
 ):
     bf16, f32 = jnp.bfloat16, jnp.float32
     experts = lax.axis_size("sp")
-    chosen = expert_ids.T[:, None, :] == jnp.arange(experts, dtype=jnp.int32)[None, :, None]
-    table = jnp.sum(jnp.where(chosen, expert_weight.T[:, None, :], 0.0), axis=0)
     tokens = queries.shape[0]
     nb = tokens // QB
-    marks = jnp.broadcast_to(doc_ids.reshape(nb, 1, QB), (nb, 8, QB))
+    marks = doc_ids.reshape(nb, 1, QB)
     half, width = residual.shape
     ff = exp_gate.shape[2]
     part = width // 4
@@ -730,7 +755,7 @@
         vm((tokens, heads), bf16),
         vm((tokens + 2 * QB, QB), bf16),
         vm((tokens + 2 * QB, QB), bf16),
-        vm((nb + 2, 8, QB), jnp.int32),
+        vm((nb + 2, 1, QB), jnp.int32),
         vm((4, tokens + 2 * QB, QB), bf16),
         vm((4, tokens + 2 * QB, QB), bf16),
         vm((half, heads), bf16),
@@ -740,6 +765,8 @@
         vm(w_out.shape, bf16),
         vm((half, width), bf16),
         vm((LINE, half, width), bf16),
+        vm(expert_ids.shape, jnp.int32),
+        vm(expert_weight.shape, f32),
         vm((LINE, experts, half), f32),
         vm((LINE, half, QB), f32),
         vm((4, width, ff), bf16),
@@ -747,6 +774,7 @@
         vm((4, 4 * ff, part), bf16),
         vm((LINE, half, 4 * ff), bf16),
         vm((half, part), f32),
+        vm((4, half, part), f32),
         vm((3, 4, half, part), bf16),
         vm((5, 4, half, part), bf16),
         vm((2, width, units), bf16),
@@ -754,10 +782,9 @@
         vm((2 * units, width), bf16),
         vm((half, 2 * units), bf16),
         vm((4, half, part), bf16),
-        dma((16,)), dma((6,)), dma((6,)), dma((3,)), dma((3,)), dma((2,)), dma((2,)),
-        dma((2,)), dma((2,)),
-        dma((6,)), dma((6,)), dma((7,)), dma((7,)), dma((5,)), dma((5,)), dma((7,)), dma((7,)),
-        dma((5,)), dma((5,)),
+        dma((17,)), dma((6,)), dma((6,)), dma((3,)), dma((3,)),
+        *[dma((2,)) for _ in range(10)],
+        *[dma((6,)) for _ in range(10)],
         dma((2, LINE, 2)), dma((LINE, 2)), dma((3, 4)), dma((5, 4)),
         dma((3,)), dma((3,)), dma((3,)), dma((3,)), dma((4,)),
     ]
@@ -765,7 +792,7 @@
     return pl.pallas_call(
         layer_kernel,
         out_shape=jax.ShapeDtypeStruct((half, width), bf16),
-        in_specs=[anyspace, anyspace, pl.BlockSpec(memory_space=pltpu.SMEM)]
+        in_specs=[anyspace] * 3 + [pl.BlockSpec(memory_space=pltpu.SMEM)]
         + [anyspace] * 5
         + [pl.BlockSpec(memory_space=pltpu.VMEM)]
         + [anyspace] * 6,
@@ -778,7 +805,7 @@
             flops=24 * rows * width * ff, bytes_accessed=32 * width * ff, transcendentals=rows * ff
         ),
     )(
-        table, marks, sink_logit, queries, keys, values, w_out, residual, ffn_gain.reshape(1, -1),
+        expert_ids, expert_weight, marks, sink_logit, queries, keys, values, w_out, residual, ffn_gain.reshape(1, -1),
         exp_gate, exp_up, exp_down, shared_gate, shared_up, shared_down,
     )
 

time: 171 us -> 171 us (level)
    unnamed x1 -> x3, local copies, waits for them, and re-layouts: 2.3 us -> 5.26 us
where the time goes in v2:
time: 171 us; the launch traced here: 170 us
  Pallas kernels  165 us (96%)
  local copies, waits for them, and re-layouts  5.26 us (3%)
    pallas_call x1, Pallas kernels, fused_shards(): pl.pallas_call(layer_kernel, out_shape=jax.ShapeDtypeStruct((half, width)...  165 us
    unnamed x3, local copies, waits for them, and re-layouts  5.26 us

profile of v2, /device:TPU:0, one launch (start us, length us, event | category | flops | bytes accessed | tf_op | source)
XLA Modules:
  0.0 169.9 jit_solution(17147865212261523509)
XLA Ops:
  0.0 1.5 copy.17.ids_in
  1.5 1.5 copy.18.wts_in
  3.0 164.7 %shard_map.154 = bf16[256,2048]{1,0:T(8,128)(2,1)} custom-call(s32[256,8]{1,0:T(8,128)} %copy.17.ids_in, f32[256,8]{1,0:T(8,128)} %copy.18.wts_in, s32[4,1,128]{2,1,0:T(1,128)} %bitcast.3, f32[8]{0:T(128)} %sink_ref.1, bf16[512,512]{1,0:T(8,128)(2,1)} %q_in.1, bf16[512,128]{1,0:T(8,128)(2,1)} %k_in.1, bf16[512,128]{1,0:T(8,128)(2,1)} %v_in.1, ...), custom_call_target="tpu_custom_call" | custom-call | flops 25769803776 | bytes 33554432 | tf_op jit(solution)/shard_map/pallas_call | solution.py:792
  167.6 2.3 %copy.20 = bf16[256,2048]{1,0:T(8,128)(2,1)} copy(bf16[256,2048]{1,0:T(8,128)(2,1)} %shard_map.154) | data formatting | bytes 2097152

commit v3 on v2

--- a/solution.py
+++ b/solution.py
@@ -614,18 +614,28 @@
     def down(b, n):
         return jnp.dot(hid[b], ds[n], preferred_element_type=f32)
 
-    def reduce_piece(step, n):
+    def reduce_piece(step, n, place=None):
         b = jnp.where(step == 2, near, line(2 + step))
         slot = jnp.where(step == 0, 3 * w, jnp.where(step == 1, 1 + w, 4 - w))
         zt = jnp.where((step == 2) & inner, zb, zf)
-        acc[...] = down(b, n)
-
-        @pl.when(inner)
-        def _():
+
+        def add():
             got(tile(step, n), rs_r.at[step, n])
-            acc[...] = acc[...] + rbuf[step, n].astype(f32)
-
-        stage[step, n] = acc[...].astype(bf16)
+            stage[step, n] = (acc[...] + rbuf[step, n].astype(f32)).astype(bf16)
+
+        if place == "end":
+            stage[step, n] = down(b, n).astype(bf16)
+        else:
+            acc[...] = down(b, n)
+            if place == "inner":
+                add()
+            else:
+                pl.when(inner)(add)
+
+                @pl.when(w == 0)
+                def _():
+                    stage[step, n] = acc[...].astype(bf16)
+
         send(
             stage.at[step, n], tile(slot, n), rs_s.at[step, n], rs_r.at[slot, n], dev(at(zt, y, c), x)
         )
@@ -639,36 +649,54 @@
         kind, j = lst[4 + k % 2]
         got(piece(held, kind, j, 3), sem.at[4 + k % 2])
 
-    def near_early(k):
+    def at_end(step, k):
         @pl.when(w == 0)
         def _():
-            reduce_piece(2, order[k])
+            reduce_piece(step, order[k], "end")
 
     down_got(0)
-    near_early(0)
+    at_end(2, 0)
     end_got(far2)
     hidden(far2, 0, 4)
+    at_end(0, 0)
     y_event(5)
     for i, (src, dst) in enumerate(zip(shared_parts, shared_views(c))):
         pend.append(send(src, dst, sx_s.at[i], sx_r.at[i], xpar))
+
+    @pl.when(inner)
+    def _():
+        hidden(far3, 0, 4)
+
     down_got(1)
-    near_early(1)
-    reduce_piece(0, order[0])
-    reduce_piece(0, order[1])
+    at_end(0, 1)
     x_event(4)
     down_got(2)
-    reduce_piece(0, order[2])
+    at_end(0, 2)
     hidden(z, 2, 4)
     x_event(5)
     down_got(3)
-    reduce_piece(0, order[3])
-    end_got(far3)
-    hidden(far3, 0, 4)
+    at_end(0, 3)
+
+    @pl.when(w == 0)
+    def _():
+        ag_got(far3, 0)
+        ag_got(far3, 1)
+        hidden(far3, 0, 4)
+
+    @pl.when(inner)
+    def _():
+        def inner_a(k, carry):
+            reduce_piece(0, nth(k), "inner")
+            return carry
+
+        lax.fori_loop(0, 4, inner_a, 0)
 
     def later(i, carry):
-        even = lax.rem(i, 2) == 0
-        step = jnp.where(inner, jnp.where(even, 1, 2), jnp.where(i < 4, 1, 2))
-        k = jnp.where(inner, i // 2, jnp.where(i < 4, i, i - 2))
+        first_two, odd = i < 2, (lax.rem(i, 2) == 1) & (i < 7)
+        in_step = jnp.where(first_two | odd, 1, 2)
+        in_k = jnp.where(first_two, i, jnp.where(odd, (i + 1) // 2, (i - 1) // 2))
+        step = jnp.where(inner, in_step, jnp.where(i < 4, 1, 2))
+        k = jnp.where(inner, in_k, jnp.where(i < 4, i, i - 3))
         reduce_piece(step, nth(k))
         return carry
 
@@ -677,9 +705,9 @@
         base[n] = res[:, cols].astype(f32) + down(z, n)
         return carry
 
-    lax.fori_loop(0, 2, later, 0)
+    lax.fori_loop(0, 1, later, 0)
     lax.fori_loop(0, 4, own_sum, 0)
-    lax.fori_loop(2, 6, later, 0)
+    lax.fori_loop(1, 6, later, 0)
 
     for i, view in enumerate(shared_views(c)):
         got(view, sx_r.at[i])
@@ -696,7 +724,7 @@
         return carry
 
     lax.fori_loop(0, 4, shared_sum, 0)
-    lax.fori_loop(6, 6 + 2 * w, later, 0)
+    lax.fori_loop(6, 7 + w, later, 0)
 
     def final(k, carry):
         n = nth(k)

time: 171 us -> 162 us (0.947)
  Pallas kernels: 165 us -> 156 us
    pallas_call x1, Pallas kernels: 165 us -> 156 us  [fused_shards(): pl.pallas_call(layer_kernel, out_shape=jax.ShapeDtypeStruct((half, width)...]
where the time goes in v3:
time: 162 us
  Pallas kernels  156 us (96%)
  local copies, waits for them, and re-layouts  5.26 us (3%)
    pallas_call x1, Pallas kernels, fused_shards(): pl.pallas_call(layer_kernel, out_shape=jax.ShapeDtypeStruct((half, width)...  156 us
    unnamed x3, local copies, waits for them, and re-layouts  5.26 us

profile of v3, /device:TPU:0, one launch (start us, length us, event | category | flops | bytes accessed | tf_op | source)
XLA Modules:
  0.0 161.6 jit_solution(11428498535965347024)
XLA Ops:
  0.0 1.5 copy.17.ids_in
  1.5 1.5 copy.18.wts_in
  3.0 156.3 %shard_map.154 = bf16[256,2048]{1,0:T(8,128)(2,1)} custom-call(s32[256,8]{1,0:T(8,128)} %copy.17.ids_in, f32[256,8]{1,0:T(8,128)} %copy.18.wts_in, s32[4,1,128]{2,1,0:T(1,128)} %bitcast.3, f32[8]{0:T(128)} %sink_ref.1, bf16[512,512]{1,0:T(8,128)(2,1)} %q_in.1, bf16[512,128]{1,0:T(8,128)(2,1)} %k_in.1, bf16[512,128]{1,0:T(8,128)(2,1)} %v_in.1, ...), custom_call_target="tpu_custom_call" | custom-call | flops 25769803776 | bytes 33554432 | tf_op jit(solution)/shard_map/pallas_call | solution.py:820
  159.2 2.3 %copy.20 = bf16[256,2048]{1,0:T(8,128)(2,1)} copy(bf16[256,2048]{1,0:T(8,128)(2,1)} %shard_map.154) | data formatting | bytes 2097152

commit v4 on v3

--- a/solution.py
+++ b/solution.py
@@ -385,11 +385,11 @@
     for cp in loads_a:
         cp.wait()
     lanes = lax.broadcasted_iota(jnp.int32, (half, QB), 1)
-    table = jnp.zeros((half, QB), f32)
-    for k in range(ids.shape[1]):
-        table = table + jnp.where(lanes == ids[:, k : k + 1], wts[:, k : k + 1], 0.0)
-    tabt[z] = table
-    tab[z] = table.T[: tab.shape[1]]
+    named = lax.broadcasted_iota(jnp.int32, tab.shape[1:], 0)
+    table = jnp.zeros(tab.shape[1:], f32)
+    for k in range(ids.shape[0]):
+        table = table + jnp.where(named == ids[k : k + 1], wts[k : k + 1], 0.0)
+    tab[z] = table
     for i, zz in enumerate(zs):
         pend.append(
             send(tab.at[z], tab.at[z], tab_s.at[i], tab_r.at[LINE - 2 - i], dev(at(zz, y, c), x))
@@ -533,8 +533,7 @@
             else:
                 ag_send(b, r, 1, bck)
 
-    def table_columns(i, carry):
-        b = lax.rem(z + i, LINE)
+    def table_columns(b, carry):
         t = tab[b]
         grown = jnp.concatenate([t, jnp.zeros((QB - t.shape[0], t.shape[1]), f32)], axis=0)
         tabt[b] = grown.T
@@ -561,7 +560,7 @@
     y_event(1)
     for i in range(LINE - 1):
         got(tab.at[z], tab_r.at[i])
-    lax.fori_loop(1, LINE, table_columns, 0)
+    lax.fori_loop(0, LINE, table_columns, 0)
     got(gs.at[1], sib_r.at[0])
     got(us.at[1], sib_r.at[1])
     hidden(z, 0, 2)
@@ -654,6 +653,11 @@
         def _():
             reduce_piece(step, order[k], "end")
 
+    def at_inner(step, k):
+        @pl.when(inner)
+        def _():
+            reduce_piece(step, order[k], "inner")
+
     down_got(0)
     at_end(2, 0)
     end_got(far2)
@@ -667,29 +671,25 @@
     def _():
         hidden(far3, 0, 4)
 
+    at_inner(0, 0)
     down_got(1)
     at_end(0, 1)
     x_event(4)
     down_got(2)
     at_end(0, 2)
+    at_inner(0, 1)
     hidden(z, 2, 4)
     x_event(5)
+    at_inner(0, 2)
     down_got(3)
     at_end(0, 3)
+    at_inner(0, 3)
 
     @pl.when(w == 0)
     def _():
         ag_got(far3, 0)
         ag_got(far3, 1)
         hidden(far3, 0, 4)
-
-    @pl.when(inner)
-    def _():
-        def inner_a(k, carry):
-            reduce_piece(0, nth(k), "inner")
-            return carry
-
-        lax.fori_loop(0, 4, inner_a, 0)
 
     def later(i, carry):
         first_two, odd = i < 2, (lax.rem(i, 2) == 1) & (i < 7)
@@ -707,7 +707,7 @@
 
     lax.fori_loop(0, 1, later, 0)
     lax.fori_loop(0, 4, own_sum, 0)
-    lax.fori_loop(1, 6, later, 0)
+    lax.fori_loop(1, 7 + w, later, 0)
 
     for i, view in enumerate(shared_views(c)):
         got(view, sx_r.at[i])
@@ -724,7 +724,6 @@
         return carry
 
     lax.fori_loop(0, 4, shared_sum, 0)
-    lax.fori_loop(6, 7 + w, later, 0)
 
     def final(k, carry):
         n = nth(k)
@@ -793,8 +792,8 @@
         vm(w_out.shape, bf16),
         vm((half, width), bf16),
         vm((LINE, half, width), bf16),
-        vm(expert_ids.shape, jnp.int32),
-        vm(expert_weight.shape, f32),
+        vm(expert_ids.shape[::-1], jnp.int32),
+        vm(expert_weight.shape[::-1], f32),
         vm((LINE, experts, half), f32),
         vm((LINE, half, QB), f32),
         vm((4, width, ff), bf16),
@@ -833,7 +832,7 @@
             flops=24 * rows * width * ff, bytes_accessed=32 * width * ff, transcendentals=rows * ff
         ),
     )(
-        expert_ids, expert_weight, marks, sink_logit, queries, keys, values, w_out, residual, ffn_gain.reshape(1, -1),
+        expert_ids.T, expert_weight.T, marks, sink_logit, queries, keys, values, w_out, residual, ffn_gain.reshape(1, -1),
         exp_gate, exp_up, exp_down, shared_gate, shared_up, shared_down,
     )
 

time: 162 us -> 149 us (0.920)
  Pallas kernels: 156 us -> 146 us
  local copies, waits for them, and re-layouts: 5.26 us -> 2.3 us
    pallas_call x1, Pallas kernels: 156 us -> 146 us  [fused_shards(): pl.pallas_call(layer_kernel, out_shape=jax.ShapeDtypeStruct((half, width)...]
    unnamed x3 -> x1, local copies, waits for them, and re-layouts: 5.26 us -> 2.3 us
where the time goes in v4:
time: 149 us
  Pallas kernels  146 us (98%)
  local copies, waits for them, and re-layouts  2.3 us (2%)
    pallas_call x1, Pallas kernels, fused_shards(): pl.pallas_call(layer_kernel, out_shape=jax.ShapeDtypeStruct((half, width)...  146 us

profile of v4, /device:TPU:0, one launch (start us, length us, event | category | flops | bytes accessed | tf_op | source)
XLA Modules:
  0.0 148.5 jit_solution(1727883417219928262)
XLA Ops:
  0.0 146.2 %shard_map.154 = bf16[256,2048]{1,0:T(8,128)(2,1)} custom-call(s32[8,256]{1,0:T(8,128)} %bitcast.4, f32[8,256]{1,0:T(8,128)} %bitcast.5, s32[4,1,128]{2,1,0:T(1,128)} %bitcast.7, f32[8]{0:T(128)} %sink_ref.1, bf16[512,512]{1,0:T(8,128)(2,1)} %q_in.1, bf16[512,128]{1,0:T(8,128)(2,1)} %k_in.1, bf16[512,128]{1,0:T(8,128)(2,1)} %v_in.1, ...), custom_call_target="tpu_custom_call" | custom-call | flops 25769803776 | bytes 33554432 | tf_op jit(solution)/shard_map/pallas_call | solution.py:819
  146.2 2.3 %copy.18 = bf16[256,2048]{1,0:T(8,128)(2,1)} copy(bf16[256,2048]{1,0:T(8,128)(2,1)} %shard_map.154) | data formatting | bytes 2097152

commit v5 on v4

--- a/solution.py
+++ b/solution.py
@@ -220,6 +220,7 @@
 QB = 128
 NEG = -1e30
 LINE = 4
+WO_PIECES = 4
 
 
 def layer_kernel(
@@ -319,9 +320,11 @@
     pend.append(send(marks_in.at[0], marks.at[nb + 1], halo_s.at[5], halo_r.at[5], prv))
 
     pair = dev(at(jnp.where(inner, zb, zf), y, c), x)
-    wrows = wo_in.shape[0] // 8
-    wpiece = lambda pos, core, i: pl.ds(pl.multiple_of(((pos * 2 + core) * 2 + i) * wrows, wrows), wrows)
-    for i in range(2):
+    wrows = wo_in.shape[0] // (4 * WO_PIECES)
+    wpiece = lambda pos, core, i: pl.ds(
+        pl.multiple_of(((pos * 2 + core) * WO_PIECES + i) * wrows, wrows), wrows
+    )
+    for i in range(WO_PIECES):
         rows = wpiece(w, c, i)
         pend.append(send(wo_in.at[rows], wo_oth.at[rows], wx_s.at[i], wx_r.at[i], xpar))
 
@@ -362,12 +365,6 @@
     y_list, x_list = own_only(x), own_only(ox)
     for i, (kind, j) in enumerate(y_list):
         pend.append(send(hbm_piece(kind, j), piece(held, kind, j, 2), y_s.at[i], y_r.at[i], ypar))
-    pend.append(send(eg_in.at[0], gs.at[1], sib_s.at[0], sib_r.at[0], sib))
-    pend.append(send(eu_in.at[0], us.at[1], sib_s.at[1], sib_r.at[1], sib))
-    for n in range(4):
-        pend.append(
-            send(hbm_piece("d", n), piece(held, "d", n, 1), sib_s.at[2 + n], sib_r.at[2 + n], sib)
-        )
 
     def y_event(i):
         kind, j = y_list[i]
@@ -384,7 +381,6 @@
 
     for cp in loads_a:
         cp.wait()
-    lanes = lax.broadcasted_iota(jnp.int32, (half, QB), 1)
     named = lax.broadcasted_iota(jnp.int32, tab.shape[1:], 0)
     table = jnp.zeros(tab.shape[1:], f32)
     for k in range(ids.shape[0]):
@@ -467,12 +463,17 @@
         attend_rows(ox * hb + i, a_out, i * QB)
         rows = pl.ds(i * QB, QB)
         pend.append(send(a_out.at[rows], a_in.at[rows], att_s.at[i], att_r.at[i], xpar))
-        if i == 0:
-            wx_event(0)
+        wx_event(i)
+    pend.append(send(eg_in.at[0], gs.at[1], sib_s.at[0], sib_r.at[0], sib))
+    pend.append(send(eu_in.at[0], us.at[1], sib_s.at[1], sib_r.at[1], sib))
+    for n in range(4):
+        pend.append(
+            send(hbm_piece("d", n), piece(held, "d", n, 1), sib_s.at[2 + n], sib_r.at[2 + n], sib)
+        )
     for i in range(hb):
         attend_rows(x * hb + i, a_own, i * QB)
-
-    wx_event(1)
+        wx_event(hb + i)
+
     y_event(0)
     for cp in loads_b:
         cp.wait()
@@ -481,11 +482,13 @@
         base[n] = res[:, cols].astype(f32) + jnp.dot(
             a_own[...], wo_own[:, cols], preferred_element_type=f32
         )
-    wz_event(0)
+    for i in range(WO_PIECES // 2):
+        wz_event(i)
     for i in range(hb):
         got(a_in.at[pl.ds(i * QB, QB)], att_r.at[i])
-    wz_event(1)
-    for i in range(2):
+    for i in range(WO_PIECES // 2, WO_PIECES):
+        wz_event(i)
+    for i in range(WO_PIECES):
         got(wo_oth.at[wpiece(w, oc, i)], wf_r.at[i])
         got(wo_oth.at[wpiece(1 - w, oc, i)], wg_r.at[i])
     square = jnp.zeros((half, 1), f32)
@@ -544,15 +547,17 @@
         b = jnp.dot(rows, up, preferred_element_type=f32)
         return a / (1.0 + jnp.exp(-a)) * b
 
-    def hidden(b, lo, hi):
+    def hidden(b, lo, hi, rows=slice(None)):
         def one(slot, carry):
             e = at(z, jnp.where(slot >= 2, oy, y), jnp.where(lax.rem(slot, 2) == 1, oc, c))
-            scale = jnp.sum(jnp.where(lanes == e, tabt[b], 0.0), axis=-1, keepdims=True)
+            weights = tabt[b, rows]
+            mine = lax.broadcasted_iota(jnp.int32, weights.shape, 1) == e
+            scale = jnp.sum(jnp.where(mine, weights, 0.0), axis=-1, keepdims=True)
             for h in range(2):
                 cols = slice(h * (ff // 2), (h + 1) * (ff // 2))
-                v = gated(tok[b], gs[slot, :, cols], us[slot, :, cols]) * scale
+                v = gated(tok[b, rows], gs[slot, :, cols], us[slot, :, cols]) * scale
                 to = pl.ds(pl.multiple_of(slot * ff + h * (ff // 2), ff // 2), ff // 2)
-                hid[b, :, to] = v.astype(bf16)
+                hid[b, rows, to] = v.astype(bf16)
             return carry
 
         lax.fori_loop(lo, hi, one, 0)
@@ -584,15 +589,26 @@
     hidden(near, 0, 2)
     x_event(2)
     relay(3, 0)
+
+    @pl.when(w == 0)
+    def _():
+        ag_got(far2, 0)
+        hidden(far2, 0, 2, slice(0, hr))
+
+    @pl.when(inner)
+    def _():
+        hidden(far2, 0, 2)
+
     y_event(4)
     x_event(3)
     relay(3, 1)
+    hidden(near, 2, 3)
     for i in range(4):
         kind, j = y_list[i]
         got(piece(held, kind, j, 3), fy_r.at[i])
         kind, j = x_list[i]
         got(piece(held, kind, j, 3), fx_r.at[i])
-    hidden(near, 2, 4)
+    hidden(near, 3, 4)
     for n in range(4):
         got(piece(held, "d", n, 1), sib_r.at[2 + n])
     srow, drow = sg_in.shape[0] // 2, sd_in.shape[0] // 2
@@ -660,8 +676,17 @@
 
     down_got(0)
     at_end(2, 0)
-    end_got(far2)
-    hidden(far2, 0, 4)
+
+    @pl.when(w == 0)
+    def _():
+        hidden(far2, 2, 4, slice(0, hr))
+        ag_got(far2, 1)
+        hidden(far2, 0, 4, slice(hr, half))
+
+    @pl.when(inner)
+    def _():
+        hidden(far2, 2, 4)
+
     at_end(0, 0)
     y_event(5)
     for i, (src, dst) in enumerate(zip(shared_parts, shared_views(c))):
@@ -707,7 +732,7 @@
 
     lax.fori_loop(0, 1, later, 0)
     lax.fori_loop(0, 4, own_sum, 0)
-    lax.fori_loop(1, 7 + w, later, 0)
+    lax.fori_loop(1, 7, later, 0)
 
     for i, view in enumerate(shared_views(c)):
         got(view, sx_r.at[i])
@@ -724,6 +749,7 @@
         return carry
 
     lax.fori_loop(0, 4, shared_sum, 0)
+    lax.fori_loop(7, 7 + w, later, 0)
 
     def final(k, carry):
         n = nth(k)
@@ -810,7 +836,8 @@
         vm((half, 2 * units), bf16),
         vm((4, half, part), bf16),
         dma((17,)), dma((6,)), dma((6,)), dma((3,)), dma((3,)),
-        *[dma((2,)) for _ in range(10)],
+        *[dma((WO_PIECES,)) for _ in range(8)],
+        dma((2,)), dma((2,)),
         *[dma((6,)) for _ in range(10)],
         dma((2, LINE, 2)), dma((LINE, 2)), dma((3, 4)), dma((5, 4)),
         dma((3,)), dma((3,)), dma((3,)), dma((3,)), dma((4,)),

time: 149 us -> 148 us (level)
  no operation moved by 1% of the time
where the time goes in v5:
time: 148 us; the launch traced here: 147 us
  Pallas kernels  145 us (98%)
  local copies, waits for them, and re-layouts  2.3 us (2%)
    pallas_call x1, Pallas kernels, fused_shards(): pl.pallas_call(layer_kernel, out_shape=jax.ShapeDtypeStruct((half, width)...  145 us

profile of v5, /device:TPU:0, one launch (start us, length us, event | category | flops | bytes accessed | tf_op | source)
XLA Modules:
  0.0 147.2 jit_solution(7792957509527316927)
XLA Ops:
  0.0 144.8 %shard_map.154 = bf16[256,2048]{1,0:T(8,128)(2,1)} custom-call(s32[8,256]{1,0:T(8,128)} %bitcast.4, f32[8,256]{1,0:T(8,128)} %bitcast.5, s32[4,1,128]{2,1,0:T(1,128)} %bitcast.7, f32[8]{0:T(128)} %sink_ref.1, bf16[512,512]{1,0:T(8,128)(2,1)} %q_in.1, bf16[512,128]{1,0:T(8,128)(2,1)} %k_in.1, bf16[512,128]{1,0:T(8,128)(2,1)} %v_in.1, ...), custom_call_target="tpu_custom_call" | custom-call | flops 25769803776 | bytes 33554432 | tf_op jit(solution)/shard_map/pallas_call | solution.py:846
  144.9 2.3 %copy.18 = bf16[256,2048]{1,0:T(8,128)(2,1)} copy(bf16[256,2048]{1,0:T(8,128)(2,1)} %shard_map.154) | data formatting | bytes 2097152

commit v6 on v5

--- a/solution.py
+++ b/solution.py
@@ -221,6 +221,8 @@
 NEG = -1e30
 LINE = 4
 WO_PIECES = 4
+TILES = 8
+CUTS = 8
 
 
 def layer_kernel(
@@ -253,7 +255,7 @@
     half = tokens // 2
     width = res_in.shape[1]
     ff = eg_in.shape[2]
-    part = width // 4
+    part = width // TILES
 
     def send(src, dst, ss, rs, to):
         cp = pltpu.make_async_remote_copy(
@@ -272,6 +274,9 @@
             src_ref=view, dst_ref=view, send_sem=ss, recv_sem=ss, device_id=sib, device_id_type=MESH
         ).wait_send()
 
+    def amount(elements):
+        return ds.at[:, pl.ds(0, elements // (TILES * part))]
+
     def load(src, dst, sem):
         cp = pltpu.make_async_copy(src, dst, sem)
         cp.start()
@@ -283,21 +288,21 @@
         load(k_in, kx.at[rows_own], loc.at[1]),
         load(v_in, vx.at[rows_own], loc.at[2]),
         load(marks_in, marks.at[pl.ds(1, tokens // QB)], loc.at[3]),
-        load(ids_in, ids, loc.at[6]),
-        load(wts_in, wts, loc.at[16]),
+        load(ids_in, ids, loc.at[4]),
+        load(wts_in, wts, loc.at[5]),
     ]
     loads_b = [
-        load(wo_in, wo_own, loc.at[4]),
-        load(res_in, res, loc.at[5]),
-        load(eg_in.at[0], gs.at[0], loc.at[7]),
-        load(eu_in.at[0], us.at[0], loc.at[8]),
-        load(sg_in, sg.at[0], loc.at[9]),
-        load(su_in, su.at[0], loc.at[10]),
-        load(sd_in, sd.at[pl.ds(0, sd_in.shape[0])], loc.at[11]),
+        load(wo_in, wo_own, loc.at[6]),
+        load(res_in, res, loc.at[7]),
+        load(eg_in.at[0], gs.at[0], loc.at[6]),
+        load(eu_in.at[0], us.at[0], loc.at[6]),
+        load(sg_in, sg.at[0], loc.at[7]),
+        load(su_in, su.at[0], loc.at[7]),
+        load(sd_in, sd.at[pl.ds(0, sd_in.shape[0])], loc.at[7]),
     ]
-    for n in range(4):
+    for n in range(TILES):
         loads_b.append(
-            load(ed_in.at[0, :, pl.ds(n * part, part)], ds.at[n, pl.ds(0, ff)], loc.at[12 + n])
+            load(ed_in.at[0, :, pl.ds(n * part, part)], ds.at[n, pl.ds(0, ff)], loc.at[6])
         )
 
     barrier = pltpu.get_barrier_semaphore()
@@ -326,20 +331,20 @@
     )
     for i in range(WO_PIECES):
         rows = wpiece(w, c, i)
-        pend.append(send(wo_in.at[rows], wo_oth.at[rows], wx_s.at[i], wx_r.at[i], xpar))
+        send(wo_in.at[rows], wo_oth.at[rows], wx_s.at[0], wx_r.at[i], xpar)
 
     def wx_event(i):
         view = wo_oth.at[wpiece(w, c, i)]
         got(view, wx_r.at[i])
-        pend.append(send(view, view, wz_s.at[i], wz_r.at[i], pair))
-        pend.append(send(view, view, wf_s.at[i], wf_r.at[i], sib))
+        send(view, view, wz_s.at[0], wz_r.at[i], pair)
+        send(view, view, wf_s.at[0], wf_r.at[0], sib)
 
     def wz_event(i):
         view = wo_oth.at[wpiece(1 - w, c, i)]
         got(view, wz_r.at[i])
-        pend.append(send(view, view, wg_s.at[i], wg_r.at[i], sib))
-
-    quarter = width // 4
+        send(view, view, wg_s.at[0], wg_r.at[0], sib)
+
+    quarter = width // CUTS
 
     def piece(refs, kind, i, slot):
         g, u, d = refs
@@ -359,25 +364,34 @@
         return ed_in.at[0, :, pl.ds(pl.multiple_of(i * part, part), part)]
 
     held = (gs, us, ds)
-    own_only = lambda v: [
-        ("g", 2 * v), ("g", 2 * v + 1), ("u", 2 * v), ("u", 2 * v + 1), ("d", v), ("d", 2 + v)
+    gates, ups = CUTS // 2, CUTS // 2 - 1
+    own_only = lambda v: [("g", gates * v + i) for i in range(gates)] + [
+        ("u", ups * v + i) for i in range(ups)
     ]
-    y_list, x_list = own_only(x), own_only(ox)
+    tiles_of = lambda v: [("d", 2 * i + v) for i in range(TILES // 2)]
+    both = [("u", i) for i in range(2 * ups, CUTS)]
+    y_list = own_only(x) + both + tiles_of(x)
+    x_list = own_only(ox) + tiles_of(ox)
+    x_gu = gates + ups
+    y_gu = x_gu + len(both)
+    relayed = {i: i if i < x_gu else i - len(both) for i in range(len(y_list)) if i < x_gu or i >= y_gu}
     for i, (kind, j) in enumerate(y_list):
-        pend.append(send(hbm_piece(kind, j), piece(held, kind, j, 2), y_s.at[i], y_r.at[i], ypar))
+        send(hbm_piece(kind, j), piece(held, kind, j, 2), y_s.at[0], y_r.at[i], ypar)
 
     def y_event(i):
         kind, j = y_list[i]
         view = piece(held, kind, j, 2)
         got(view, y_r.at[i])
-        pend.append(send(view, view, x_s.at[i], x_r.at[i], xpar))
-        pend.append(send(view, piece(held, kind, j, 3), fy_s.at[i], fy_r.at[i], sib))
+        if i in relayed:
+            k = relayed[i]
+            send(view, view, x_s.at[0], x_r.at[k], xpar)
+        send(view, piece(held, kind, j, 3), fy_s.at[0], fy_r.at[max(0, i - y_gu + 1)], sib)
 
     def x_event(i):
         kind, j = x_list[i]
         view = piece(held, kind, j, 2)
         got(view, x_r.at[i])
-        pend.append(send(view, piece(held, kind, j, 3), fx_s.at[i], fx_r.at[i], sib))
+        send(view, piece(held, kind, j, 3), fx_s.at[0], fx_r.at[max(0, i - x_gu + 1)], sib)
 
     for cp in loads_a:
         cp.wait()
@@ -462,37 +476,33 @@
     for i in range(hb):
         attend_rows(ox * hb + i, a_out, i * QB)
         rows = pl.ds(i * QB, QB)
-        pend.append(send(a_out.at[rows], a_in.at[rows], att_s.at[i], att_r.at[i], xpar))
+        send(a_out.at[rows], a_in.at[rows], att_s.at[0], att_r.at[0], xpar)
         wx_event(i)
-    pend.append(send(eg_in.at[0], gs.at[1], sib_s.at[0], sib_r.at[0], sib))
-    pend.append(send(eu_in.at[0], us.at[1], sib_s.at[1], sib_r.at[1], sib))
-    for n in range(4):
-        pend.append(
-            send(hbm_piece("d", n), piece(held, "d", n, 1), sib_s.at[2 + n], sib_r.at[2 + n], sib)
-        )
+    send(eg_in.at[0], gs.at[1], sib_s.at[0], sib_r.at[0], sib)
+    send(eu_in.at[0], us.at[1], sib_s.at[0], sib_r.at[1], sib)
+    for n in range(TILES):
+        send(hbm_piece("d", n), piece(held, "d", n, 1), sib_s.at[0], sib_r.at[2], sib)
     for i in range(hb):
         attend_rows(x * hb + i, a_own, i * QB)
         wx_event(hb + i)
 
     y_event(0)
-    for cp in loads_b:
-        cp.wait()
-    for n in range(4):
+    first_loads = wo_in.size + 3 * eg_in.size
+    for i, elements in ((6, first_loads), (7, res_in.size + 3 * sg_in.size)):
+        view = amount(elements)
+        pltpu.make_async_copy(view, view, loc.at[i]).wait()
+    for n in range(TILES):
         cols = slice(n * part, (n + 1) * part)
         base[n] = res[:, cols].astype(f32) + jnp.dot(
             a_own[...], wo_own[:, cols], preferred_element_type=f32
         )
-    for i in range(WO_PIECES // 2):
+    for i in range(WO_PIECES):
         wz_event(i)
-    for i in range(hb):
-        got(a_in.at[pl.ds(i * QB, QB)], att_r.at[i])
-    for i in range(WO_PIECES // 2, WO_PIECES):
-        wz_event(i)
-    for i in range(WO_PIECES):
-        got(wo_oth.at[wpiece(w, oc, i)], wf_r.at[i])
-        got(wo_oth.at[wpiece(1 - w, oc, i)], wg_r.at[i])
+    got(a_in, att_r.at[0])
+    got(amount(wo_in.size // 4), wf_r.at[0])
+    got(amount(wo_in.size // 4), wg_r.at[0])
     square = jnp.zeros((half, 1), f32)
-    for n in range(4):
+    for n in range(TILES):
         cols = slice(n * part, (n + 1) * part)
         r = (
             base[n] + jnp.dot(a_in[...], wo_oth[:, cols], preferred_element_type=f32)
@@ -502,7 +512,7 @@
         square = square + jnp.sum(rf * rf, axis=-1, keepdims=True)
     inv = lax.rsqrt(square * (1.0 / width) + norm_eps)
     for n in range(4):
-        cols = slice(n * part, (n + 1) * part)
+        cols = slice(n * (width // 4), (n + 1) * (width // 4))
         tok[z, :, cols] = (res[:, cols].astype(f32) * inv * gain_ref[:, cols]).astype(bf16)
 
     hr = half // 2
@@ -510,10 +520,7 @@
 
     def ag_send(b, r, direction, to):
         view = tok.at[b, rows_of(r)]
-        send(view, view, ag_s.at[direction, b, r], ag_r.at[b, r], to)
-
-    def ag_sent(b, r, direction):
-        sent(tok.at[b, rows_of(r)], ag_s.at[direction, b, r])
+        send(view, view, ag_s.at[direction], ag_r.at[b, r], to)
 
     def ag_got(b, r):
         got(tok.at[b, rows_of(r)], ag_r.at[b, r])
@@ -532,9 +539,9 @@
         def _():
             ag_got(b, r)
             if ob == 0:
-                ag_send(b, r, 0, fwd)
+                ag_send(b, r, 2, fwd)
             else:
-                ag_send(b, r, 1, bck)
+                ag_send(b, r, 3, bck)
 
     def table_columns(b, carry):
         t = tab[b]
@@ -568,15 +575,20 @@
     lax.fori_loop(0, LINE, table_columns, 0)
     got(gs.at[1], sib_r.at[0])
     got(us.at[1], sib_r.at[1])
+    y_event(2)
     hidden(z, 0, 2)
+    y_event(3)
+    x_event(0)
     relay(0, 0)
     relay(2, 0)
-    x_event(0)
-    y_event(2)
     x_event(1)
+    y_event(4)
+    x_event(2)
+    y_event(5)
     relay(0, 1)
     relay(2, 1)
-    y_event(3)
+    x_event(3)
+    y_event(6)
     near, far2, far3 = line(1 - w), line(2), line(3)
 
     def end_got(b):
@@ -587,7 +599,10 @@
 
     end_got(near)
     hidden(near, 0, 2)
-    x_event(2)
+    x_event(4)
+    y_event(7)
+    x_event(5)
+    y_event(8)
     relay(3, 0)
 
     @pl.when(w == 0)
@@ -599,18 +614,14 @@
     def _():
         hidden(far2, 0, 2)
 
-    y_event(4)
-    x_event(3)
-    relay(3, 1)
+    x_event(6)
+    y_event(9)
     hidden(near, 2, 3)
-    for i in range(4):
-        kind, j = y_list[i]
-        got(piece(held, kind, j, 3), fy_r.at[i])
-        kind, j = x_list[i]
-        got(piece(held, kind, j, 3), fx_r.at[i])
+    cut = quarter * ff
+    got(amount(y_gu * cut), fy_r.at[0])
+    got(amount(x_gu * cut), fx_r.at[0])
     hidden(near, 3, 4)
-    for n in range(4):
-        got(piece(held, "d", n, 1), sib_r.at[2 + n])
+    got(amount(ed_in.size), sib_r.at[2])
     srow, drow = sg_in.shape[0] // 2, sd_in.shape[0] // 2
     shared_views = lambda core: [
         sg.at[1, pl.ds(core * srow, srow)],
@@ -623,7 +634,7 @@
         sd_in.at[pl.ds(c * drow, drow)],
     ]
 
-    order = [x, 2 + x, ox, 2 + ox]
+    order = [2 * (k // 2) + (x if k % 2 == 0 else ox) for k in range(TILES)]
     tile = lambda slot, n: rbuf.at[slot, n]
 
     def down(b, n):
@@ -652,17 +663,16 @@
                     stage[step, n] = acc[...].astype(bf16)
 
         send(
-            stage.at[step, n], tile(slot, n), rs_s.at[step, n], rs_r.at[slot, n], dev(at(zt, y, c), x)
+            stage.at[step, n], tile(slot, n), rs_s.at[step], rs_r.at[slot, n], dev(at(zt, y, c), x)
         )
 
     def nth(k):
-        base_n = jnp.where(k < 2, x, ox)
-        return base_n + 2 * lax.rem(k, 2)
+        return 2 * (k // 2) + jnp.where(lax.rem(k, 2) == 0, x, ox)
 
     def down_got(k):
-        lst, sem = (y_list, fy_r) if k < 2 else (x_list, fx_r)
-        kind, j = lst[4 + k % 2]
-        got(piece(held, kind, j, 3), sem.at[4 + k % 2])
+        lst, sem, first_d = (y_list, fy_r, y_gu) if k % 2 == 0 else (x_list, fx_r, x_gu)
+        kind, j = lst[first_d + k // 2]
+        got(piece(held, kind, j, 3), sem.at[1 + k // 2])
 
     def at_end(step, k):
         @pl.when(w == 0)
@@ -674,12 +684,24 @@
         def _():
             reduce_piece(step, order[k], "inner")
 
+    early = TILES // 2
     down_got(0)
     at_end(2, 0)
 
     @pl.when(w == 0)
     def _():
         hidden(far2, 2, 4, slice(0, hr))
+
+    x_event(7)
+    down_got(1)
+    at_end(2, 1)
+    y_event(10)
+    down_got(2)
+    at_end(2, 2)
+    relay(3, 1)
+
+    @pl.when(w == 0)
+    def _():
         ag_got(far2, 1)
         hidden(far2, 0, 4, slice(hr, half))
 
@@ -687,41 +709,70 @@
     def _():
         hidden(far2, 2, 4)
 
-    at_end(0, 0)
-    y_event(5)
+    for k in range(early - 1):
+        at_end(0, k)
+    x_event(8)
+    y_event(11)
+    down_got(3)
+    at_end(2, 3)
+    at_end(0, 3)
+
+    @pl.when(inner)
+    def _():
+        hidden(far3, 0, 4)
+
+    y_event(12)
     for i, (src, dst) in enumerate(zip(shared_parts, shared_views(c))):
-        pend.append(send(src, dst, sx_s.at[i], sx_r.at[i], xpar))
+        send(src, dst, sx_s.at[0], sx_r.at[0], xpar)
+    x_event(9)
+
+    def a_tiles(k, carry):
+        reduce_piece(0, nth(k), "inner")
+        return carry
 
     @pl.when(inner)
     def _():
-        hidden(far3, 0, 4)
-
-    at_inner(0, 0)
-    down_got(1)
-    at_end(0, 1)
-    x_event(4)
-    down_got(2)
-    at_end(0, 2)
-    at_inner(0, 1)
+        lax.fori_loop(0, 2, a_tiles, 0)
+
+    for k in range(4, 7):
+        down_got(k)
+        at_end(0, k)
+
+    @pl.when(inner)
+    def _():
+        lax.fori_loop(2, 4, a_tiles, 0)
+
     hidden(z, 2, 4)
-    x_event(5)
-    at_inner(0, 2)
-    down_got(3)
-    at_end(0, 3)
-    at_inner(0, 3)
 
     @pl.when(w == 0)
     def _():
         ag_got(far3, 0)
+        hidden(far3, 0, 4, slice(0, hr))
+
+    x_event(10)
+    down_got(7)
+    at_end(0, 7)
+
+    @pl.when(inner)
+    def _():
+        lax.fori_loop(4, TILES, a_tiles, 0)
+
+    @pl.when(w == 0)
+    def _():
         ag_got(far3, 1)
-        hidden(far3, 0, 4)
+        hidden(far3, 0, 4, slice(hr, half))
+
+    lag = 3
+    turns = 2 * TILES - lag
 
     def later(i, carry):
-        first_two, odd = i < 2, (lax.rem(i, 2) == 1) & (i < 7)
-        in_step = jnp.where(first_two | odd, 1, 2)
-        in_k = jnp.where(first_two, i, jnp.where(odd, (i + 1) // 2, (i - 1) // 2))
-        step = jnp.where(inner, in_step, jnp.where(i < 4, 1, 2))
-        k = jnp.where(inner, in_k, jnp.where(i < 4, i, i - 3))
+        odd = lax.rem(i - lag, 2) == 0
+        far = (i < lag) | ((i < turns) & ~odd)
+        in_step = jnp.where(far, 1, 2)
+        far_k = jnp.where(i < lag, i, (i + lag - 1) // 2)
+        near_k = jnp.where(i < turns, (i - lag) // 2, i - TILES)
+        step = jnp.where(inner, in_step, jnp.where(i < TILES, 1, 2))
+        k = jnp.where(inner, jnp.where(far, far_k, near_k), jnp.where(i < TILES, i, i - TILES + early))
         reduce_piece(step, nth(k))
         return carry
 
@@ -730,15 +781,39 @@
         base[n] = res[:, cols].astype(f32) + down(z, n)
         return carry
 
-    lax.fori_loop(0, 1, later, 0)
-    lax.fori_loop(0, 4, own_sum, 0)
-    lax.fori_loop(1, 7, later, 0)
-
-    for i, view in enumerate(shared_views(c)):
-        got(view, sx_r.at[i])
-        pend.append(send(view, view, ss_s.at[i], ss_r.at[i], sib))
-    for i, view in enumerate(shared_views(oc)):
-        got(view, ss_r.at[i])
+    at_once = 2 * TILES - early
+
+    block = half * width
+
+    def drain():
+        for cp in pend:
+            cp.wait_send()
+        for sem, elements in (
+            (wx_s, wo_in.size // 4), (wz_s, wo_in.size // 4), (wf_s, wo_in.size // 4),
+            (wg_s, wo_in.size // 4), (att_s, a_out.size), (sib_s, 3 * eg_in.size),
+            (y_s, len(y_list) * cut), (x_s, len(x_list) * cut), (fy_s, len(y_list) * cut),
+            (fx_s, len(x_list) * cut), (ag_s, block),
+        ):
+            sent(amount(elements), sem.at[0])
+
+    @pl.when(inner)
+    def _():
+        drain()
+        for i, elements in ((1, block), (2, block), (3, 2 * block)):
+            sent(amount(elements), ag_s.at[i])
+
+    lax.fori_loop(0, 2, later, 0)
+    lax.fori_loop(0, TILES, own_sum, 0)
+    middle = at_once + w
+    lax.fori_loop(2, middle, later, 0)
+    pl.when(w == 0)(drain)
+
+    shared_size = 3 * sg_in.size // 2
+    got(amount(shared_size), sx_r.at[0])
+    for view in shared_views(c):
+        send(view, view, ss_s.at[0], ss_r.at[0], sib)
+    lax.fori_loop(middle, at_once + early * w, later, 0)
+    got(amount(shared_size), ss_r.at[0])
     units = sg_in.shape[1]
     for h in range(2):
         sh[:, h * units : (h + 1) * units] = gated(tok[z], sg[h], su[h]).astype(bf16)
@@ -748,8 +823,7 @@
         base[n] = base[n] + jnp.dot(sh[...], sd[:, cols], preferred_element_type=f32)
         return carry
 
-    lax.fori_loop(0, 4, shared_sum, 0)
-    lax.fori_loop(7, 7 + w, later, 0)
+    lax.fori_loop(0, TILES, shared_sum, 0)
 
     def final(k, carry):
         n = nth(k)
@@ -763,28 +837,20 @@
             acc[...] = acc[...] + rbuf[4, n].astype(f32)
 
         ost[n] = acc[...].astype(bf16)
-        load(ost.at[n], out_ref.at[:, cols], out_sem.at[n])
+        load(ost.at[n], out_ref.at[:, cols], out_sem.at[0])
         return carry
 
-    lax.fori_loop(0, 4, final, 0)
-
-    for cp in pend:
-        cp.wait_send()
-    for r in range(2):
-        ag_sent(z, r, 0)
-
-        @pl.when(inner)
-        def _():
-            ag_sent(z, r, 1)
-            ag_sent(line(0), r, 0)
-            ag_sent(line(2), r, 1)
-            ag_sent(line(3), r, 1)
-
-    for step in range(3):
-        for n in range(4):
-            sent(stage.at[step, n], rs_s.at[step, n])
-    for n in range(4):
-        pltpu.make_async_copy(ost.at[n], out_ref.at[:, pl.ds(n * part, part)], out_sem.at[n]).wait()
+    def steps_sent(steps):
+        for step in steps:
+            sent(amount(block), rs_s.at[step])
+
+    steps_sent((0, 1))
+    lax.fori_loop(0, TILES, final, 0)
+
+    sent(amount(shared_size), sx_s.at[0])
+    sent(amount(shared_size), ss_s.at[0])
+    steps_sent((2,))
+    pltpu.make_async_copy(amount(block), amount(block), out_sem.at[0]).wait()
 
 
 def fused_shards(
@@ -798,7 +864,7 @@
     marks = doc_ids.reshape(nb, 1, QB)
     half, width = residual.shape
     ff = exp_gate.shape[2]
-    part = width // 4
+    part = width // TILES
     units = shared_gate.shape[1]
     heads = queries.shape[1]
     vm = pltpu.VMEM
@@ -824,23 +890,25 @@
         vm((LINE, half, QB), f32),
         vm((4, width, ff), bf16),
         vm((4, width, ff), bf16),
-        vm((4, 4 * ff, part), bf16),
+        vm((TILES, 4 * ff, part), bf16),
         vm((LINE, half, 4 * ff), bf16),
         vm((half, part), f32),
-        vm((4, half, part), f32),
-        vm((3, 4, half, part), bf16),
-        vm((5, 4, half, part), bf16),
+        vm((TILES, half, part), f32),
+        vm((3, TILES, half, part), bf16),
+        vm((5, TILES, half, part), bf16),
         vm((2, width, units), bf16),
         vm((2, width, units), bf16),
         vm((2 * units, width), bf16),
         vm((half, 2 * units), bf16),
-        vm((4, half, part), bf16),
-        dma((17,)), dma((6,)), dma((6,)), dma((3,)), dma((3,)),
-        *[dma((WO_PIECES,)) for _ in range(8)],
-        dma((2,)), dma((2,)),
-        *[dma((6,)) for _ in range(10)],
-        dma((2, LINE, 2)), dma((LINE, 2)), dma((3, 4)), dma((5, 4)),
-        dma((3,)), dma((3,)), dma((3,)), dma((3,)), dma((4,)),
+        vm((TILES, half, part), bf16),
+        dma((8,)), dma((6,)), dma((6,)), dma((3,)), dma((3,)),
+        dma((1,)), dma((WO_PIECES,)), dma((1,)), dma((WO_PIECES,)),
+        *[dma((1,)) for _ in range(6)],
+        dma((1,)), dma((3,)),
+        dma((1,)), dma((CUTS + 1 + TILES // 2,)), dma((1,)), dma((CUTS - 1 + TILES // 2,)),
+        dma((1,)), dma((1 + TILES // 2,)), dma((1,)), dma((1 + TILES // 2,)),
+        dma((4,)), dma((LINE, 2)), dma((3,)), dma((5, TILES)),
+        dma((1,)), dma((1,)), dma((1,)), dma((1,)), dma((1,)),
     ]
     rows = LINE * half
     return pl.pallas_call(

time: 148 us -> 146 us (0.986)
  Pallas kernels: 145 us -> 143 us
    pallas_call x1, Pallas kernels: 145 us -> 143 us  [fused_shards(): pl.pallas_call(layer_kernel, out_shape=jax.ShapeDtypeStruct((half, width)...]
where the time goes in v6:
time: 146 us; the launch traced here: 145 us
  Pallas kernels  143 us (98%)
  local copies, waits for them, and re-layouts  2.3 us (2%)
    pallas_call x1, Pallas kernels, fused_shards(): pl.pallas_call(layer_kernel, out_shape=jax.ShapeDtypeStruct((half, width)...  143 us

profile of v6, /device:TPU:0, one launch (start us, length us, event | category | flops | bytes accessed | tf_op | source)
XLA Modules:
  0.0 145.5 jit_solution(6949130881568018219)
XLA Ops:
  0.0 143.1 %shard_map.154 = bf16[256,2048]{1,0:T(8,128)(2,1)} custom-call(s32[8,256]{1,0:T(8,128)} %bitcast.4, f32[8,256]{1,0:T(8,128)} %bitcast.5, s32[4,1,128]{2,1,0:T(1,128)} %bitcast.7, f32[8]{0:T(128)} %sink_ref.1, bf16[512,512]{1,0:T(8,128)(2,1)} %q_in.1, bf16[512,128]{1,0:T(8,128)(2,1)} %k_in.1, bf16[512,128]{1,0:T(8,128)(2,1)} %v_in.1, ...), custom_call_target="tpu_custom_call" | custom-call | flops 25769803776 | bytes 33554432 | tf_op jit(solution)/shard_map/pallas_call | solution.py:914
  143.1 2.3 %copy.18 = bf16[256,2048]{1,0:T(8,128)(2,1)} copy(bf16[256,2048]{1,0:T(8,128)(2,1)} %shard_map.154) | data formatting | bytes 2097152

commit v7 on v6

--- a/solution.py
+++ b/solution.py
@@ -753,9 +753,16 @@
     down_got(7)
     at_end(0, 7)
 
+    def own_sum(n, carry):
+        cols = pl.ds(pl.multiple_of(n * part, part), part)
+        base[n] = res[:, cols].astype(f32) + down(z, n)
+        return carry
+
     @pl.when(inner)
     def _():
-        lax.fori_loop(4, TILES, a_tiles, 0)
+        lax.fori_loop(4, 5, a_tiles, 0)
+        lax.fori_loop(0, TILES, own_sum, 0)
+        lax.fori_loop(5, TILES, a_tiles, 0)
 
     @pl.when(w == 0)
     def _():
@@ -776,11 +783,6 @@
         reduce_piece(step, nth(k))
         return carry
 
-    def own_sum(n, carry):
-        cols = pl.ds(pl.multiple_of(n * part, part), part)
-        base[n] = res[:, cols].astype(f32) + down(z, n)
-        return carry
-
     at_once = 2 * TILES - early
 
     block = half * width
@@ -803,7 +805,11 @@
             sent(amount(elements), ag_s.at[i])
 
     lax.fori_loop(0, 2, later, 0)
-    lax.fori_loop(0, TILES, own_sum, 0)
+
+    @pl.when(w == 0)
+    def _():
+        lax.fori_loop(0, TILES, own_sum, 0)
+
     middle = at_once + w
     lax.fori_loop(2, middle, later, 0)
     pl.when(w == 0)(drain)

time: 146 us -> 145 us (level)
  no operation moved by 1% of the time
where the time goes in v7:
time: 145 us
  Pallas kernels  143 us (99%)
  local copies, waits for them, and re-layouts  2.3 us (2%)
    pallas_call x1, Pallas kernels, fused_shards(): pl.pallas_call(layer_kernel, out_shape=jax.ShapeDtypeStruct((half, width)...  143 us

profile of v7, /device:TPU:0, one launch (start us, length us, event | category | flops | bytes accessed | tf_op | source)
XLA Modules:
  0.0 145.2 jit_solution(2708544940339751911)
XLA Ops:
  0.0 142.9 %shard_map.154 = bf16[256,2048]{1,0:T(8,128)(2,1)} custom-call(s32[8,256]{1,0:T(8,128)} %bitcast.4, f32[8,256]{1,0:T(8,128)} %bitcast.5, s32[4,1,128]{2,1,0:T(1,128)} %bitcast.7, f32[8]{0:T(128)} %sink_ref.1, bf16[512,512]{1,0:T(8,128)(2,1)} %q_in.1, bf16[512,128]{1,0:T(8,128)(2,1)} %k_in.1, bf16[512,128]{1,0:T(8,128)(2,1)} %v_in.1, ...), custom_call_target="tpu_custom_call" | custom-call | flops 25769803776 | bytes 33554432 | tf_op jit(solution)/shard_map/pallas_call | solution.py:920
  142.9 2.3 %copy.18 = bf16[256,2048]{1,0:T(8,128)(2,1)} copy(bf16[256,2048]{1,0:T(8,128)(2,1)} %shard_map.154) | data formatting | bytes 2097152
